TPU v7x, 32 devices: a whole 2x2x4 slice. The times are simulated.
32 devices in a mesh: ep: 8 (over z, core), tp: 4 (over y, x).
Axes of the slice: x: 2, y: 2, z: 4, core: 2. Of those that a mesh axis runs over, the one named last changes fastest.
Arguments:
- mixer_value_input: bfloat16 [2048, 4096], P('ep', 'tp'), may hold values from -6 to 6
- input_state_matrix: bfloat16 [2048, 2048], P('ep', 'tp'), may hold values from -6 to 6
- output_state_matrix: bfloat16 [2048, 2048], P('ep', 'tp'), may hold values from -6 to 6
- output_gate_input: bfloat16 [2048, 4096], P('ep', 'tp'), may hold values from -6 to 6
- step_input: float32 [2048, 64], P('ep', 'tp'), may hold values from -6 to -2
- extra_log_decay: float32 [2048, 64], P('ep', 'tp'), may hold values from -1 to 0
- head_log_decay: float32 [64], P('tp'), may hold values from -10 to 1
- head_skip_scale: float32 [64], P('tp'), may hold values from 0.5 to 2
- value_kernel: float32 [4, 4096], P(None, 'tp'), may hold values from -3 to 3
- input_matrix_kernel: float32 [4, 2048], P(None, 'tp'), may hold values from -3 to 3
- output_matrix_kernel: float32 [4, 2048], P(None, 'tp'), may hold values from -3 to 3
- mixer_norm_scale: float32 [4096], P('tp'), may hold values from 0.1 to 1.9
- mixer_output_weight: bfloat16 [4096, 2048], P(None, 'tp'), may hold values from -0.09375 to 0.09375
- second_token_rows: bfloat16 [2048, 2048], P('ep'), may hold values from -6 to 6
- expert_norm_scale: float32 [2048], replicated, may hold values from 0.1 to 1.9
- routed_expert_index: int32 [2048, 4], P('ep'), may hold values from 0 to 15, all different within a row; in each aligned block of 256 rows (0 to 255, 256 to 511, ...) at most 96 rows name the same one
- routed_expert_weight: float32 [2048, 4], P('ep'), may hold values from 0.1 to 1
- routed_gate_weight: bfloat16 [16, 2048, 1024], P('ep', None, 'tp'), may hold values from -0.125 to 0.125
- routed_up_weight: bfloat16 [16, 2048, 1024], P('ep', None, 'tp'), may hold values from -0.125 to 0.125
- routed_down_weight: bfloat16 [16, 1024, 2048], P('ep', None, 'tp'), may hold values from -0.1875 to 0.1875
- shared_gate_weight: bfloat16 [2048, 1024], P(None, 'tp'), may hold values from -0.125 to 0.125
- shared_up_weight: bfloat16 [2048, 1024], P(None, 'tp'), may hold values from -0.125 to 0.125
- shared_down_weight: bfloat16 [1024, 2048], P(None, 'tp'), may hold values from -0.1875 to 0.1875
Outputs:
- mixer_output: bfloat16 [2048, 2048], P('ep', 'tp')
- routed_out: bfloat16 [2048, 2048], P('ep', 'tp')
Inputs may be any that keep to these rules, and one draw needn't show every extreme that they name: `routed_expert_index`: in each aligned block of 256 rows (the rows of one index of ep) no expert is named more than 96 times, a bound that some block reaches.
All inputs are finite; a program needn't handle non-finite values.
Results may differ from a plain program's by a relative error of at most 0.012.
Values may be sent and summed in bfloat16 or wider, within the bound.
A program may use at most 64 MiB of HBM per device.

v0:
```python
import jax
import jax.numpy as jnp
from jax import lax
from jax.sharding import PartitionSpec as P

HEAD_DIM = 64
STATE = 128
CONV_TAPS = 4
BLOCK = 128
TOP_K = 4


epsilon = 1e-05
precise = lax.Precision.HIGHEST


def passed_along(x, axis, by):
    size = lax.axis_size(axis)
    pairs = [(i, i + by) for i in range(size) if 0 <= i + by < size]
    return lax.ppermute(x, axis, pairs)


def carried_in(total_log, state, axis):
    size = lax.axis_size(axis)
    place = lax.axis_index(axis)
    log = passed_along(total_log, axis, 1)
    hold = passed_along(state.astype(jnp.bfloat16), axis, 1).astype(jnp.float32)
    by = 1
    while by < size - 1:
        before = passed_along(hold.astype(jnp.bfloat16), axis, by).astype(jnp.float32)
        hold = hold + jnp.exp(log)[:, None, None] * before
        log = log + passed_along(log, axis, by)
        by *= 2
    return hold


def conv_silu(tail_rows, source, weights):
    length = source.shape[0]
    padded = jnp.concatenate([tail_rows, source], axis=0)
    total_sum = jnp.zeros(source.shape, jnp.float32)
    for tap_index in range(CONV_TAPS):
        total_sum = (
            total_sum
            + padded[tap_index : tap_index + length].astype(jnp.float32) * weights[tap_index]
        )
    return jax.nn.silu(total_sum).astype(jnp.bfloat16)


def carry_blocks(carried, inputs):
    block_decay, block_state = inputs
    return (carried * block_decay[:, None, None] + block_state, carried)


def earlier_counts(mask, rows):
    at = jnp.arange(rows)
    tri = (at[:, None] < at[None, :]).astype(jnp.bfloat16)
    return lax.dot_general(
        mask.astype(jnp.bfloat16),
        tri,
        (((mask.ndim - 1,), (0,)), ((), ())),
        preferred_element_type=jnp.float32,
    )


def on_device(
    mixer_value_input,
    input_state_matrix,
    output_state_matrix,
    output_gate_input,
    step_input,
    extra_log_decay,
    head_log_decay,
    head_skip_scale,
    value_kernel,
    input_matrix_kernel,
    output_matrix_kernel,
    mixer_norm_scale,
    mixer_output_weight,
    second_token_rows,
    expert_norm_scale,
    routed_expert_index,
    routed_expert_weight,
    routed_gate_weight,
    routed_up_weight,
    routed_down_weight,
    shared_gate_weight,
    shared_up_weight,
    shared_down_weight,
):
    length = mixer_value_input.shape[0]
    heads_local = step_input.shape[1]
    width_x = mixer_value_input.shape[1]
    width_b = input_state_matrix.shape[1]
    groups_local = width_b // STATE
    head_ratio = heads_local // groups_local
    nblocks = length // BLOCK
    lead_row = length - CONV_TAPS + 1
    edge_rows = jnp.concatenate(
        [
            mixer_value_input[lead_row:],
            input_state_matrix[lead_row:],
            output_state_matrix[lead_row:],
        ],
        axis=1,
    )
    tail_rows = passed_along(edge_rows, "ep", 1)
    rows_local = second_token_rows.shape[0]
    model_width = second_token_rows.shape[1]
    local_experts = routed_gate_weight.shape[0]
    ep_count = lax.axis_size("ep")
    experts = local_experts * ep_count
    capacity = max(2, 3 * rows_local * TOP_K // (2 * experts))
    col_width = model_width // lax.axis_size("tp")
    rows_wide = second_token_rows.astype(jnp.float32)
    normed = (
        rows_wide
        * lax.rsqrt(jnp.mean(rows_wide * rows_wide, axis=-1, keepdims=True) + epsilon)
        * expert_norm_scale
    ).astype(jnp.bfloat16)
    ids = routed_expert_index.T.astype(jnp.float32)
    id_rows = -(-ids.size // col_width)
    id_block = jnp.pad(
        ids.astype(jnp.bfloat16).reshape(-1), (0, id_rows * col_width - ids.size)
    ).reshape(id_rows, col_width)
    id_block = jnp.pad(id_block, ((0, -id_rows % 8), (0, 0)))
    my_columns = lax.dynamic_slice_in_dim(normed, lax.axis_index("tp") * col_width, col_width, 1)
    outgoing, value_rows, in_rows, out_rows = lax.optimization_barrier(
        (
            jnp.concatenate([my_columns, id_block], axis=0),
            mixer_value_input,
            input_state_matrix,
            output_state_matrix,
        )
    )
    everyone = lax.all_gather(outgoing, "ep", axis=0)
    values = conv_silu(tail_rows[:, :width_x], value_rows, value_kernel)
    in_mat = conv_silu(
        tail_rows[:, width_x : width_x + width_b], in_rows, input_matrix_kernel
    )
    out_mat = conv_silu(
        tail_rows[:, width_x + width_b :], out_rows, output_matrix_kernel
    )
    step_length = jax.nn.softplus(step_input)
    decay_logarithm = -jnp.exp(head_log_decay)[None, :] * step_length + extra_log_decay
    running = jnp.cumsum(decay_logarithm.reshape(nblocks, BLOCK, heads_local), axis=1)
    value_wide = values.astype(jnp.float32).reshape(nblocks, BLOCK, heads_local, HEAD_DIM)
    scaled = value_wide * step_length.reshape(nblocks, BLOCK, heads_local)[..., None]
    in_blocks = in_mat.reshape(nblocks, BLOCK, groups_local, STATE)
    out_blocks = out_mat.reshape(nblocks, BLOCK, groups_local, STATE)
    scores = jnp.einsum(
        "bign,bjgn->bgij", out_blocks, in_blocks, preferred_element_type=jnp.float32
    )
    scores = jnp.repeat(scores, head_ratio, axis=1)
    spread = jnp.transpose(running[:, :, None, :] - running[:, None, :, :], (0, 3, 1, 2))
    lower_mask = jnp.tril(jnp.ones((BLOCK, BLOCK), bool))[None, None]
    decay_mat = jnp.where(lower_mask, jnp.exp(jnp.where(lower_mask, spread, 0.0)), 0.0)
    inside = jnp.einsum("bhij,bjhp->bihp", scores * decay_mat, scaled, precision=precise)
    out_head = jnp.repeat(out_blocks.astype(jnp.float32), head_ratio, axis=2)
    in_head = jnp.repeat(in_blocks.astype(jnp.float32), head_ratio, axis=2)
    block_logs = running[:, -1]
    to_end = jnp.exp(block_logs[:, None, :] - running)
    block_state = jnp.einsum("bjhn,bjh,bjhp->bhpn", in_head, to_end, scaled, precision=precise)
    start_state = jnp.zeros((heads_local, HEAD_DIM, STATE), jnp.float32)
    local_total, local_prev = lax.scan(
        carry_blocks, start_state, (jnp.exp(block_logs), block_state)
    )
    before_logs = jnp.cumsum(block_logs, axis=0) - block_logs
    everyone, local_total = lax.optimization_barrier((everyone, local_total))
    incoming = carried_in(jnp.sum(block_logs, axis=0), local_total, "ep")
    their_rows = everyone[:, :rows_local]
    their_ids = everyone[:, rows_local : rows_local + id_rows].reshape(ep_count, -1)
    their_ids = their_ids[:, : ids.size].reshape(ep_count, TOP_K, rows_local).astype(jnp.float32)
    mine = (lax.axis_index("ep") * local_experts + jnp.arange(local_experts)).astype(jnp.float32)
    named = jnp.any(their_ids[:, None] == mine[None, :, None, None], axis=2)
    seat = jnp.where(named, earlier_counts(named, rows_local), -1.0)
    seats = jnp.arange(capacity, dtype=jnp.float32)
    pick = (seat[:, :, None, :] == seats[None, None, :, None]).astype(jnp.bfloat16)
    arrived = jnp.stack(
        [
            jnp.einsum(
                "bsr,brd->bsd", pick[:, j], their_rows, preferred_element_type=jnp.float32
            )
            .astype(jnp.bfloat16)
            .reshape(ep_count * capacity, col_width)
            for j in range(local_experts)
        ]
    )
    column_piece = lax.all_gather(arrived, "tp", axis=2, tiled=True)
    column_piece, incoming = lax.optimization_barrier((column_piece, incoming))
    entering = local_prev + jnp.exp(before_logs)[:, :, None, None] * incoming[None]
    carried_term = (
        jnp.einsum("bihn,bhpn->bihp", out_head, entering, precision=precise)
        * jnp.exp(running)[..., None]
    )
    mixed_heads = (inside + carried_term).reshape(length, heads_local, HEAD_DIM)
    mixed_heads = mixed_heads + head_skip_scale[None, :, None] * value_wide.reshape(
        length, heads_local, HEAD_DIM
    )
    gated_heads = mixed_heads * jax.nn.silu(output_gate_input.astype(jnp.float32)).reshape(
        length, heads_local, HEAD_DIM
    )
    grouped = gated_heads.reshape(length, groups_local, head_ratio * HEAD_DIM)
    grouped = grouped * lax.rsqrt(jnp.mean(grouped * grouped, axis=-1, keepdims=True) + epsilon)
    mixer_normed = (grouped.reshape(length, width_x) * mixer_norm_scale).astype(jnp.bfloat16)
    gate_pre = jnp.einsum(
        "esd,edf->esf", column_piece, routed_gate_weight, preferred_element_type=jnp.float32
    )
    up_pre = jnp.einsum(
        "esd,edf->esf", column_piece, routed_up_weight, preferred_element_type=jnp.float32
    )
    hidden = (jax.nn.silu(gate_pre) * up_pre).astype(jnp.bfloat16)
    shared_hidden = (
        jax.nn.silu(jnp.dot(normed, shared_gate_weight, preferred_element_type=jnp.float32))
        * jnp.dot(normed, shared_up_weight, preferred_element_type=jnp.float32)
    ).astype(jnp.bfloat16)
    whole_hidden = lax.all_gather(hidden, "tp", axis=2, tiled=True)
    both = lax.all_gather(
        jnp.concatenate([mixer_normed, shared_hidden], axis=1), "tp", axis=1, tiled=True
    ).reshape(length, lax.axis_size("tp"), -1)
    whole_mix = both[:, :, :width_x].reshape(length, -1)
    whole_shared = both[:, :, width_x:].reshape(length, -1)
    mixer_output = jnp.dot(
        whole_mix, mixer_output_weight, preferred_element_type=jnp.float32
    ).astype(jnp.bfloat16)
    expert_result = jnp.einsum(
        "esf,efd->esd", whole_hidden, routed_down_weight, preferred_element_type=jnp.float32
    ).astype(jnp.bfloat16)
    going = jnp.concatenate(
        [expert_result[j].reshape(ep_count, capacity, col_width) for j in range(local_experts)],
        axis=1,
    )
    returned = lax.all_to_all(going, "ep", split_axis=0, concat_axis=0, tiled=True)
    returned = returned.reshape(experts * capacity, col_width)
    kinds = jnp.arange(experts, dtype=jnp.float32)
    chosen = ids[:, None, :] == kinds[None, :, None]
    count = earlier_counts(jnp.any(chosen, axis=0), rows_local)
    position = jnp.sum(jnp.where(chosen, count[None], 0.0), axis=1)
    slot = (ids * capacity + position).T.astype(jnp.int32)
    columns = jnp.arange(experts * capacity, dtype=jnp.int32)[None, :]
    spread = jnp.zeros((rows_local, experts * capacity), jnp.float32)
    for k in range(TOP_K):
        spread = spread + jnp.where(
            slot[:, k : k + 1] == columns, routed_expert_weight[:, k : k + 1], 0.0
        )
    high = lax.reduce_precision(spread, 8, 7)
    low = (spread - high).astype(jnp.bfloat16)
    routed_sum = jnp.dot(
        high.astype(jnp.bfloat16), returned, preferred_element_type=jnp.float32
    ) + jnp.dot(low, returned, preferred_element_type=jnp.float32)
    shared_result = jnp.dot(whole_shared, shared_down_weight, preferred_element_type=jnp.float32)
    routed_out = (routed_sum + shared_result).astype(jnp.bfloat16)
    return (mixer_output, routed_out)


def solution(mesh):
    return jax.shard_map(
        on_device,
        mesh=mesh,
        in_specs=(
            P("ep", "tp"),
            P("ep", "tp"),
            P("ep", "tp"),
            P("ep", "tp"),
            P("ep", "tp"),
            P("ep", "tp"),
            P("tp"),
            P("tp"),
            P(None, "tp"),
            P(None, "tp"),
            P(None, "tp"),
            P("tp"),
            P(None, "tp"),
            P("ep", None),
            P(),
            P("ep", None),
            P("ep", None),
            P("ep", None, "tp"),
            P("ep", None, "tp"),
            P("ep", None, "tp"),
            P(None, "tp"),
            P(None, "tp"),
            P(None, "tp"),
        ),
        out_specs=(P("ep", "tp"), P("ep", "tp")),
        check_vma=False,
    )
```

profile of v0, /device:TPU:0, one launch (start us, length us, event | category | flops | bytes accessed | tf_op | source)
XLA Modules:
  0.0 239.8 jit_solution(12581473368572431942)
XLA Ops:
  10.7 3.2 %collective-permute-start = (bf16[3,2048]{0,1:T(8,128)(2,1)}, bf16[3,2048]{0,1:T(8,128)(2,1)}, u32[]{:S(2)}, u32[]{:S(2)}) collective-permute-start(bf16[3,2048]{0,1:T(8,128)(2,1)} %copy.77), channel_id=1, source_target_pairs={{0,4},{4,8},{8,12},{12,16},{16,20},{20,24},{24,28},{1,5},{5,9},{9,... | collective-permute-start | bytes 36872 | tf_op jit(solution)/shard_map/ppermute | solution.py:20
  26.7 3.4 %multiply_convert_fusion.2 = (bf16[256,512]{1,0:T(8,128)(2,1)}, bf16[256,512]{1,0:T(8,128)(2,1)}) fusion(bf16[256,512]{1,0:T(8,128)(2,1)} %param.26, bf16[3,512]{1,0:T(4,128)(2,1)} %copy.81, f32[512]{0:T(512)} %bitcast.141, f32[512]{0:T(512)} %bitcast.142, f32[512]{0:T(512)} %bitcast.140, f32[512]{0:T(512)} %bitcast.139, f32[512]{0:T(512)} %bitcast.145, ...), kind=kLoop, calls=%fused_computation.103 | loop fusion | flops 6553600 | bytes 1071104 | tf_op jit(solution)/shard_map/convert_element_type | solution.py:46
  32.9 2.9 %fusion.71 = f32[256,1024]{0,1:T(8,128)} fusion(f32[1024]{0:T(1024)} %bitcast.134, bf16[256,1024]{0,1:T(8,128)(2,1)S(1)} %copy.78, f32[1024]{0:T(1024)} %bitcast.135, bf16[3,1024]{0,1:T(8,128)(2,1)S(1)} %slice.176, f32[1024]{0:T(1024)} %bitcast.133, f32[1024]{0:T(1024)} %bitcast.132), kind=kLoop, calls=%fused_computation.106 | loop fusion | flops 6815744 | bytes 1595392 | tf_op jit(solution)/shard_map/convert_element_type | solution.py:146
  35.8 2.7 %reshape.132 = f32[2,128,16,64]{1,0,3,2:T(2,128)} reshape(f32[256,1024]{0,1:T(8,128)} %fusion.71) | data formatting | bytes 2097152 | tf_op jit(solution)/shard_map/reshape | solution.py:146
  38.6 3.0 %broadcast_multiply_fusion = (f32[2,128,16,64]{1,0,3,2:T(2,128)S(1)}, f32[2,128,16,64]{1,0,3,2:T(2,128)}) fusion(f32[2,128,16]{1,0,2:T(2,128)S(1)} %copy.88, f32[2,128,16,64]{1,0,3,2:T(2,128)} %reshape.132, f32[2,128,16]{1,0,2:T(2,128)} %mul.326), kind=kLoop, calls=%fused_computation.102 | loop fusion | flops 524288 | bytes 3178496 | tf_op jit(solution)/shard_map/bjhn,bjh,bjhp->bhpn/dot_general | solution.py:162
  41.8 3.1 %fusion.37 = f32[2,16,64,128]{3,2,1,0:T(8,128)} fusion(f32[2,128,16,128]{3,1,2,0:T(8,128)S(1)} %bitcast.120, f32[2,128,16,64]{1,0,3,2:T(2,128)S(1)} %get-tuple-element.78), kind=kOutput, calls=%fused_computation.55 | convolution fusion | flops 402653184 | bytes 4194304 | tf_op jit(solution)/shard_map/bjhn,bjh,bjhp->bhpn/dot_general | solution.py:162
  44.9 4.0 %while.13 = (s32[]{:T(128)}, f32[16,64,128]{2,1,0:T(8,128)S(1)}, f32[2,16,64,128]{3,2,1,0:T(8,128)}, f32[2,16]{1,0:T(2,128)S(1)}, f32[2,16,64,128]{3,2,1,0:T(8,128)}, /*index=5*/s32[]{:T(128)}, s32[]{:T(128)}) while((s32[]{:T(128)}, f32[16,64,128]{2,1,0:T(8,128)S(1)}, f32[2,16,64,128]{3,2,1,0:T(8,128)}, f32[2,16]{1,0:T(2,128)S(1)}, ...), condition=%wide.region_3.4_spmd.clone, body=%wide.region_2.3_spmd.clone.sunk | while | flops 524291 | bytes 2621740 | solution.py:164
  55.5 3.0 %collective-permute-start.1 = (bf16[16,64,128]{2,1,0:T(8,128)(2,1)S(1)}, bf16[16,64,128]{2,1,0:T(8,128)(2,1)S(1)}, u32[]{:S(2)}, u32[]{:S(2)}) collective-permute-start(bf16[16,64,128]{2,1,0:T(8,128)(2,1)S(1)} %convert_element_type.179), channel_id=1, source_target_pairs={{0,4},{4,8},{8,12},{12,16},{16,20},{20,24},{24,28},{1,5},{5,9},{9,... | collective-permute-start | bytes 786440 | tf_op jit(solution)/shard_map/ppermute | solution.py:20
  59.7 4.5 %collective-permute-start.3 = (bf16[16,64,128]{2,1,0:T(8,128)(2,1)S(1)}, bf16[16,64,128]{2,1,0:T(8,128)(2,1)S(1)}, u32[]{:S(2)}, u32[]{:S(2)}) collective-permute-start(bf16[16,64,128]{2,1,0:T(8,128)(2,1)S(1)} %collective-permute-done.1), channel_id=1, source_target_pairs={{0,4},{4,8},{8,12},{12,16},{16,20},{20,24},{24,28},{1,5},{5,9},{9,... | collective-permute-start | bytes 786440 | tf_op jit(solution)/shard_map/ppermute | solution.py:20
  64.2 4.4 %collective-permute-start.2 = (f32[16]{0:T(128)S(1)}, f32[16]{0:T(128)S(1)}, u32[]{:S(2)}, u32[]{:S(2)}) collective-permute-start(f32[16]{0:T(128)S(1)} %copy-done.31), channel_id=1, source_target_pairs={{0,4},{4,8},{8,12},{12,16},{16,20},{20,24},{24,28},{1,5},{5,9},{9,... | collective-permute-start | bytes 200 | tf_op jit(solution)/shard_map/ppermute | solution.py:20
  72.9 6.5 %collective-permute-start.5 = (bf16[16,64,128]{2,1,0:T(8,128)(2,1)S(1)}, bf16[16,64,128]{2,1,0:T(8,128)(2,1)S(1)}, u32[]{:S(2)}, u32[]{:S(2)}) collective-permute-start(bf16[16,64,128]{2,1,0:T(8,128)(2,1)S(1)} %fusion.72), channel_id=1, source_target_pairs={{0,8},{4,12},{8,16},{12,20},{16,24},{20,28},{1,9},{5,13},{9,17},{1... | collective-permute-start | bytes 786440 | tf_op jit(solution)/shard_map/ppermute | solution.py:20
  79.4 4.6 %collective-permute-done.5 = bf16[16,64,128]{2,1,0:T(8,128)(2,1)S(1)} collective-permute-done((bf16[16,64,128]{2,1,0:T(8,128)(2,1)S(1)}, bf16[16,64,128]{2,1,0:T(8,128)(2,1)S(1)}, u32[]{:S(2)}, u32[]{:S(2)}) %collective-permute-start.5) | collective-permute-done | bytes 262176 | tf_op jit(solution)/shard_map/ppermute | solution.py:20
  84.3 5.4 %collective-permute-start.7 = (bf16[16,64,128]{2,1,0:T(8,128)(2,1)S(1)}, bf16[16,64,128]{2,1,0:T(8,128)(2,1)S(1)}, u32[]{:S(2)}, u32[]{:S(2)}) collective-permute-start(bf16[16,64,128]{2,1,0:T(8,128)(2,1)S(1)} %fusion.74), channel_id=1, source_target_pairs={{0,16},{4,20},{8,24},{12,28},{1,17},{5,21},{9,25},{13,29},{2,18},{... | collective-permute-start | bytes 786440 | tf_op jit(solution)/shard_map/ppermute | solution.py:20
  95.3 31.1 %all-gather.6.cloned.1.call-done = bf16[2,768,2048]{2,1,0:T(8,128)(2,1)} async-done(((bf16[2,768,512]{2,1,0:T(8,128)(2,1)}), bf16[2,768,2048]{2,1,0:T(8,128)(2,1)}) %all-gather.6.cloned.1.call-update) | async-done | bytes 6291472 | tf_op jit(solution)/shard_map/all_gather | solution.py:188
  126.4 5.3 %fusion.101 = f32[2,768,256]{2,1,0:T(8,128)S(1)} fusion(bf16[2,768,2048]{2,1,0:T(8,128)(2,1)} %all-gather.6.cloned.1.call-done, bf16[2,2048,256]{2,1,0:T(8,128)(2,1)} %param.42), kind=kOutput, calls=%fused_computation.161 | convolution fusion | flops 1610612736 | bytes 9961472 | tf_op jit(solution)/shard_map/esd,edf->esf/dot_general | solution.py:205
  132.2 2.9 %multiply_convert_fusion = bf16[2,768,256]{2,1,0:T(8,128)(2,1)} fusion(f32[2,768,256]{2,1,0:T(8,128)S(1)} %fusion.101, bf16[2,768,2048]{2,1,0:T(8,128)(2,1)S(1)} %copy-done.33, bf16[2,2048,256]{2,1,0:T(8,128)(2,1)S(1)} %copy-done.35), kind=kOutput, calls=%fused_computation.25 | convolution fusion | flops 1612972032 | bytes 10747904 | tf_op jit(solution)/shard_map/esd,edf->esf/dot_general | solution.py:208
  146.3 4.2 %fusion.27 = f32[2,128,16,64]{1,3,2,0:T(8,128)S(1)} fusion(f32[2,128,16,128]{3,1,2,0:T(8,128)S(1)} %bitcast.121, f32[2,16,64,128]{3,2,1,0:T(8,128)S(1)} %copy-done.11, f32[2,128,16]{1,2,0:T(8,128)S(1)} %copy-done.13, f32[16,64,128]{2,1,0:T(8,128)S(1)} %copy-done.9, f32[2,16]{1,0:T(2,128)S(1)} %copy-done.27), kind=kOutput, calls=%fused_computation.37 | convolution fusion | flops 403439616 | bytes 4735104 | tf_op jit(solution)/shard_map/bihn,bhpn->bihp/dot_general | solution.py:192
  151.7 4.2 %fusion.24 = f32[2,128,16,64]{1,3,2,0:T(8,128)S(1)} fusion(f32[2,128,16,64]{1,3,2,0:T(8,128)S(1)} %fusion.27, f32[2,16,128,128]{3,2,1,0:T(8,128)S(1)} %bitcast.119, f32[2,128,16,64]{1,0,3,2:T(2,128)S(1)} %copy-done.6, f32[2,16,128]{2,1,0:T(8,128)S(1)} %copy.85, pred[128,128]{1,0:T(8,128)(4,1)S(1)} %copy-done.12), kind=kOutput, calls=%fused_computation.35 | convolution fusion | flops 405012480 | bytes 5275648 | tf_op jit(solution)/shard_map/bhij,bjhp->bihp/dot_general | solution.py:157
  157.7 3.2 %reshape.140 = f32[256,4,256]{0,2,1:T(8,128)} reshape(f32[2,128,16,64]{1,0,3,2:T(2,128)} %copy.94) | data formatting | bytes 2097152 | tf_op jit(solution)/shard_map/reshape | solution.py:195
  164.4 14.7 %all-gather.10.cloned.1.call-done = bf16[2,768,1024]{2,1,0:T(8,128)(2,1)} async-done(((bf16[2,768,256]{2,1,0:T(8,128)(2,1)}), bf16[2,768,1024]{2,1,0:T(8,128)(2,1)}) %all-gather.10.cloned.1.call-update) | async-done | bytes 3145744 | tf_op jit(solution)/shard_map/all_gather | solution.py:216
  179.0 3.7 %convolution_convert_fusion = bf16[2,768,512]{2,1,0:T(8,128)(2,1)S(1)} fusion(bf16[2,768,1024]{2,1,0:T(8,128)(2,1)} %all-gather.10.cloned.1.call-done, bf16[2,1024,512]{2,1,0:T(8,128)(2,1)S(1)} %copy-done), kind=kOutput, calls=%fused_computation.21 | convolution fusion | flops 1611399168 | bytes 6815744 | tf_op jit(solution)/shard_map/esf,efd->esd/dot_general | solution.py:225
  184.4 4.7 %all-to-all-start = ((bf16[8,192,512]{2,1,0:T(8,128)(2,1)}), bf16[8,192,512]{2,1,0:T(8,128)(2,1)}, u32[]{:S(2)}, u32[]{:S(2)}) async-start(bf16[8,192,512]{2,1,0:T(8,128)(2,1)} %pad_maximum_fusion.1), calls=%async_computation | async-start | bytes 3145728 | tf_op jit(solution)/shard_map/all_to_all | solution.py:232
  189.4 30.9 %all-gather.8.cloned.1.call-done = bf16[256,5120]{0,1:T(8,128)(2,1)} async-done(((bf16[256,1280]{0,1:T(8,128)(2,1)}), bf16[256,5120]{0,1:T(8,128)(2,1)}) %all-gather.8.cloned.1.call-update) | async-done | bytes 2621456 | tf_op jit(solution)/shard_map/all_gather | solution.py:217
  229.5 2.6 %convolution_add_fusion.1 = f32[256,512]{1,0:T(8,128)S(1)} fusion(f32[256,512]{1,0:T(8,128)S(1)} %fusion.47, bf16[1536,512]{1,0:T(8,128)(2,1)} %bitcast.43, f32[256]{0:T(256)S(1)} %bitcast.152, s32[256]{0:T(256)S(1)} %bitcast.158, f32[256]{0:T(256)S(1)} %bitcast.154, s32[256]{0:T(256)S(1)} %bitcast.160, f32[256]{0:T(256)S(1)} %bitcast.150, ...), kind=kOutput, calls=%fused_computation.41 | convolution fusion | flops 408289280 | bytes 2629632 | tf_op jit(solution)/shard_map/dot_general | solution.py:249
  (185 shorter events, 71.0 us)
Async XLA Ops:
  7.2 171.9 %copy-start = (bf16[2,1024,512]{2,1,0:T(8,128)(2,1)S(1)}, bf16[2,1024,512]{2,1,0:T(8,128)(2,1)}, u32[]{:S(2)}) copy-start(bf16[2,1024,512]{2,1,0:T(8,128)(2,1)} %param.44) | copy-start | bytes 6291460
  7.2 8.8 %copy-start.7 = (bf16[256,2048]{1,0:T(8,128)(2,1)S(1)}, bf16[256,2048]{1,0:T(8,128)(2,1)}, u32[]{:S(2)}) copy-start(bf16[256,2048]{1,0:T(8,128)(2,1)} %param.38) | copy-start | bytes 3145732
  7.2 8.2 %copy-start.17 = (s32[256,4]{0,1:T(4,128)S(1)}, s32[256,4]{0,1:T(4,128)}, u32[]{:S(2)}) copy-start(s32[256,4]{0,1:T(4,128)} %param.40) | copy-start | bytes 12292
  7.2 8.8 %copy-start.22 = (f32[2048]{0:T(1024)S(1)}, f32[2048]{0:T(1024)}, u32[]{:S(2)}) copy-start(f32[2048]{0:T(1024)} %param.39) | copy-start | bytes 24580
  7.2 42.7 %all-gather.12.cloned.1.call-start = ((), (), s32[]{:S(2)}) async-start(), calls=%async_computation.4 | async-start | bytes 2433024 | tf_op jit(solution)/shard_map/all_gather | solution.py:135
  10.7 14.2 %collective-permute-start = (bf16[3,2048]{0,1:T(8,128)(2,1)}, bf16[3,2048]{0,1:T(8,128)(2,1)}, u32[]{:S(2)}, u32[]{:S(2)}) collective-permute-start(bf16[3,2048]{0,1:T(8,128)(2,1)} %copy.77), channel_id=1, source_target_pairs={{0,4},{4,8},{8,12},{12,16},{16,20},{20,24},{24,28},{1,5},{5,9},{9,... | collective-permute-start | bytes 36872 | tf_op jit(solution)/shard_map/ppermute | solution.py:20
  16.1 5.0 %copy-start.19 = (f32[4,1024]{1,0:T(4,128)S(1)}, f32[4,1024]{1,0:T(4,128)}, u32[]{:S(2)}) copy-start(f32[4,1024]{1,0:T(4,128)} %param.33) | copy-start | bytes 49156
  18.2 108.2 %all-gather.6.cloned.1.call-start = ((), (), s32[]{:S(2)}) async-start(), calls=%async_computation.1 | async-start | bytes 7864320 | tf_op jit(solution)/shard_map/all_gather | solution.py:188
  44.9 5.9 %copy-start.29 = (f32[2]{0:T(128)S(1)}, f32[2]{0:T(128)}, u32[]{:S(2)}) copy-start(f32[2]{0:T(128)} %add_convert_fusion) | copy-start | bytes 28
  55.4 8.8 %copy-start.31 = (f32[16]{0:T(128)S(1)}, f32[16]{0:T(128)}, u32[]{:S(2)}) copy-start(f32[16]{0:T(128)} %get-tuple-element.84) | copy-start | bytes 196
  55.4 123.6 %all-gather.10.cloned.1.call-start = ((), (), s32[]{:S(2)}) async-start(), calls=%async_computation.3 | async-start | bytes 3932160 | tf_op jit(solution)/shard_map/all_gather | solution.py:216
  55.5 4.1 %collective-permute-start.1 = (bf16[16,64,128]{2,1,0:T(8,128)(2,1)S(1)}, bf16[16,64,128]{2,1,0:T(8,128)(2,1)S(1)}, u32[]{:S(2)}, u32[]{:S(2)}) collective-permute-start(bf16[16,64,128]{2,1,0:T(8,128)(2,1)S(1)} %convert_element_type.179), channel_id=1, source_target_pairs={{0,4},{4,8},{8,12},{12,16},{16,20},{20,24},{24,28},{1,5},{5,9},{9,... | collective-permute-start | bytes 786440 | tf_op jit(solution)/shard_map/ppermute | solution.py:20
  59.7 13.1 %collective-permute-start.3 = (bf16[16,64,128]{2,1,0:T(8,128)(2,1)S(1)}, bf16[16,64,128]{2,1,0:T(8,128)(2,1)S(1)}, u32[]{:S(2)}, u32[]{:S(2)}) collective-permute-start(bf16[16,64,128]{2,1,0:T(8,128)(2,1)S(1)} %collective-permute-done.1), channel_id=1, source_target_pairs={{0,4},{4,8},{8,12},{12,16},{16,20},{20,24},{24,28},{1,5},{5,9},{9,... | collective-permute-start | bytes 786440 | tf_op jit(solution)/shard_map/ppermute | solution.py:20
  64.2 5.2 %collective-permute-start.2 = (f32[16]{0:T(128)S(1)}, f32[16]{0:T(128)S(1)}, u32[]{:S(2)}, u32[]{:S(2)}) collective-permute-start(f32[16]{0:T(128)S(1)} %copy-done.31), channel_id=1, source_target_pairs={{0,4},{4,8},{8,12},{12,16},{16,20},{20,24},{24,28},{1,5},{5,9},{9,... | collective-permute-start | bytes 200 | tf_op jit(solution)/shard_map/ppermute | solution.py:20
  69.4 3.3 %collective-permute-start.4 = (f32[16]{0:T(128)S(1)}, f32[16]{0:T(128)S(1)}, u32[]{:S(2)}, u32[]{:S(2)}) collective-permute-start(f32[16]{0:T(128)S(1)} %collective-permute-done.2), channel_id=1, source_target_pairs={{0,4},{4,8},{8,12},{12,16},{16,20},{20,24},{24,28},{1,5},{5,9},{9,... | collective-permute-start | bytes 200 | tf_op jit(solution)/shard_map/ppermute | solution.py:20
  72.9 11.1 %collective-permute-start.5 = (bf16[16,64,128]{2,1,0:T(8,128)(2,1)S(1)}, bf16[16,64,128]{2,1,0:T(8,128)(2,1)S(1)}, u32[]{:S(2)}, u32[]{:S(2)}) collective-permute-start(bf16[16,64,128]{2,1,0:T(8,128)(2,1)S(1)} %fusion.72), channel_id=1, source_target_pairs={{0,8},{4,12},{8,16},{12,20},{16,24},{20,28},{1,9},{5,13},{9,17},{1... | collective-permute-start | bytes 786440 | tf_op jit(solution)/shard_map/ppermute | solution.py:20
  84.3 9.9 %collective-permute-start.7 = (bf16[16,64,128]{2,1,0:T(8,128)(2,1)S(1)}, bf16[16,64,128]{2,1,0:T(8,128)(2,1)S(1)}, u32[]{:S(2)}, u32[]{:S(2)}) collective-permute-start(bf16[16,64,128]{2,1,0:T(8,128)(2,1)S(1)} %fusion.74), channel_id=1, source_target_pairs={{0,16},{4,20},{8,24},{12,28},{1,17},{5,21},{9,25},{13,29},{2,18},{... | collective-permute-start | bytes 786440 | tf_op jit(solution)/shard_map/ppermute | solution.py:20
  89.7 4.5 %collective-permute-start.6 = (f32[16]{0:T(128)S(1)}, f32[16]{0:T(128)S(1)}, u32[]{:S(2)}, u32[]{:S(2)}) collective-permute-start(f32[16]{0:T(128)S(1)} %get-tuple-element.77), channel_id=1, source_target_pairs={{0,8},{4,12},{8,16},{12,20},{16,24},{20,28},{1,9},{5,13},{9,17},{1... | collective-permute-start | bytes 200 | tf_op jit(solution)/shard_map/ppermute | solution.py:20
  126.4 5.4 %copy-start.33 = (bf16[2,768,2048]{2,1,0:T(8,128)(2,1)S(1)}, bf16[2,768,2048]{2,1,0:T(8,128)(2,1)}, u32[]{:S(2)}) copy-start(bf16[2,768,2048]{2,1,0:T(8,128)(2,1)} %all-gather.6.cloned.1.call-done) | copy-start | bytes 18874372
  126.4 5.8 %copy-start.35 = (bf16[2,2048,256]{2,1,0:T(8,128)(2,1)S(1)}, bf16[2,2048,256]{2,1,0:T(8,128)(2,1)}, u32[]{:S(2)}) copy-start(bf16[2,2048,256]{2,1,0:T(8,128)(2,1)} %param.43) | copy-start | bytes 6291460
  135.1 5.9 %copy-start.4 = (bf16[256,2048]{1,0:T(8,128)(2,1)S(1)}, bf16[256,2048]{1,0:T(8,128)(2,1)}, u32[]{:S(2)}) copy-start(bf16[256,2048]{1,0:T(8,128)(2,1)} %copy-done.3) | copy-start | bytes 3145732
  135.2 85.1 %all-gather.8.cloned.1.call-start = ((), (), s32[]{:S(2)}) async-start(), calls=%async_computation.2 | async-start | bytes 3276800 | tf_op jit(solution)/shard_map/all_gather | solution.py:217
  184.4 5.0 %copy-start.18 = (s32[256,4]{0,1:T(4,128)S(1)}, s32[256,4]{0,1:T(4,128)}, u32[]{:S(2)}) copy-start(s32[256,4]{0,1:T(4,128)} %param.40) | copy-start | bytes 12292
  184.4 42.6 %all-to-all-start = ((bf16[8,192,512]{2,1,0:T(8,128)(2,1)}), bf16[8,192,512]{2,1,0:T(8,128)(2,1)}, u32[]{:S(2)}, u32[]{:S(2)}) async-start(bf16[8,192,512]{2,1,0:T(8,128)(2,1)} %pad_maximum_fusion.1), calls=%async_computation | async-start | bytes 3145728 | tf_op jit(solution)/shard_map/all_to_all | solution.py:232
  (27 other events, 67.0 us)
Sparse Core Ops, SparseCore 0:
  18.4 31.4 all-gather.11
  55.5 70.8 all-gather.5
  135.3 43.6 all-gather.9
  180.7 39.4 all-gather.7
where the time goes:
time: 241 us; the launch traced here: 240 us
  waiting for transfers between devices  87.8 us (36%)
  matrix products  37.4 us (16%)
  starting transfers between devices  36.9 us (15%)
  local copies, waits for them, and re-layouts  34.6 us (14%)
  other arithmetic  28.6 us (12%)
  between operations  14.4 us (6%)
    ppermute x8, starting transfers between devices, passed_along(): return lax.ppermute(x, axis, pairs)  32 us
    all_gather x1, waiting for transfers between devices, on_device(): column_piece = lax.all_gather(arrived, 'tp', axis=2, tiled=True)  31.1 us
    all_gather x1, waiting for transfers between devices, on_device(): lax.all_gather(jnp.concatenate([mixer_normed, shared_hidden], axis=1), 't...  30.9 us
    all_gather x1, waiting for transfers between devices, on_device(): whole_hidden = lax.all_gather(hidden, 'tp', axis=2, tiled=True)  14.7 us
    ppermute x8, waiting for transfers between devices, passed_along(): return lax.ppermute(x, axis, pairs)  9.39 us
    unnamed x77, local copies, waits for them, and re-layouts  6.78 us
    dot_general x1, matrix products, on_device(): jnp.einsum('esd,edf->esf', column_piece, routed_gate_weight, preferred_el...  5.34 us
  transfers between devices with their start and end apart: 13, of which 10 were waited for; matrix products, arithmetic and copies ran while one was open for 30% of the time, Pallas kernels for 0%

commit v1 on v0

--- a/solution.py
+++ b/solution.py
@@ -1,6 +1,11 @@
+import functools
+import types
+
 import jax
 import jax.numpy as jnp
 from jax import lax
+from jax.experimental import pallas as pl
+from jax.experimental.pallas import tpu as pltpu
 from jax.sharding import PartitionSpec as P
 
 HEAD_DIM = 64
@@ -252,9 +257,641 @@
     return (mixer_output, routed_out)
 
 
+MESH = pl.DeviceIdType.MESH
+HALO = 16
+LANES = 128
+
+
+def silu(v):
+    return v / (1.0 + jnp.exp(-v))
+
+
+def dot(a, b, contract=((1,), (0,)), exact=False):
+    return lax.dot_general(
+        a,
+        b,
+        (contract, ((), ())),
+        precision=precise if exact else None,
+        preferred_element_type=jnp.float32,
+    )
+
+
+def iota(shape, axis):
+    return lax.broadcasted_iota(jnp.int32, shape, axis)
+
+
+def at(start, size):
+    return pl.ds(pl.multiple_of(start, size), size)
+
+
+def body(dims, names, *refs):
+    r = types.SimpleNamespace(**dict(zip(names, refs)))
+    n_ep, rows, cap, ratio = dims.n_ep, dims.rows, dims.cap, dims.ratio
+    nz = n_ep // 2
+    half = rows // 2
+    tp = dims.tp
+    quarter = dims.quarter
+    heads, groups, width = dims.heads, dims.groups, dims.width
+    band = ratio * HEAD_DIM
+    ff, sff = dims.ff, dims.sff
+    f32, bf16 = jnp.float32, jnp.bfloat16
+
+    e, t = lax.axis_index("ep"), lax.axis_index("tp")
+    z, c = lax.div(e, 2), lax.rem(e, 2)
+    other = 1 - c
+    partner = e + 1 - 2 * c
+    tx = t + 1 - 2 * lax.rem(t, 2)
+    ty = lax.rem(t + 2, tp)
+    td = tp - 1 - t
+
+    def remote(src, dst, send, recv, to):
+        return pltpu.make_async_remote_copy(
+            src_ref=src, dst_ref=dst, send_sem=send, recv_sem=recv, device_id=to, device_id_type=MESH
+        )
+
+    fetched = dims.fetched
+
+    def fetch(name):
+        return pltpu.make_async_copy(
+            getattr(r, name), getattr(r, "v_" + name), r.local_sem.at[fetched.index(name)]
+        )
+
+    for name in fetched:
+        fetch(name).start()
+
+    def got(*wanted):
+        for name in wanted:
+            fetch(name).wait()
+
+    barrier = pltpu.get_barrier_semaphore()
+    for by in range(1, n_ep):
+        pl.semaphore_signal(barrier, inc=1, device_id=(lax.rem(e + by, n_ep), t), device_id_type=MESH)
+    for to in (tx, ty):
+        pl.semaphore_signal(barrier, inc=1, device_id=(e, to), device_id_type=MESH)
+
+    def zsource(k):
+        return lax.rem(z + k, nz)
+
+    def plane(buf, send, recv):
+        def leg(q, piece, slot, to):
+            return remote(buf(q, piece), buf(q, piece), send(slot), recv(slot), (e, to))
+
+        def start():
+            leg(t, 0, 0, tx).start()
+            leg(t, 1, 3, ty).start()
+            leg(t, 1, 1, tx).start()
+            leg(t, 0, 2, ty).start()
+
+        def relay():
+            leg(tx, 0, 0, tx).wait_recv()
+            leg(tx, 0, 4, ty).start()
+            leg(ty, 1, 3, ty).wait_recv()
+            leg(ty, 1, 5, tx).start()
+
+        def finish():
+            leg(tx, 1, 1, tx).wait_recv()
+            leg(ty, 0, 2, ty).wait_recv()
+            leg(td, 0, 4, ty).wait_recv()
+            leg(td, 1, 5, tx).wait_recv()
+
+        def drain():
+            leg(t, 0, 0, tx).wait_send()
+            leg(t, 1, 1, tx).wait_send()
+            leg(t, 0, 2, ty).wait_send()
+            leg(t, 1, 3, ty).wait_send()
+            leg(tx, 0, 4, ty).wait_send()
+            leg(ty, 1, 5, tx).wait_send()
+
+        return types.SimpleNamespace(start=start, relay=relay, finish=finish, drain=drain)
+
+    def tokens(k):
+        block = 2 * zsource(k) + c
+        return plane(
+            lambda q, piece: r.tok.at[block, q, pl.ds(piece * half, half)],
+            lambda slot: r.tok_send.at[k, slot],
+            lambda slot: r.tok_recv.at[k, slot],
+        )
+
+    def hiddens(k):
+        return plane(
+            lambda q, piece: r.hid.at[k, q, pl.ds(piece * 2 * cap, 2 * cap)],
+            lambda slot: r.hid_send.at[k, slot],
+            lambda slot: r.hid_recv.at[k, slot],
+        )
+
+    mixes = plane(
+        lambda q, piece: r.mix.at[q, pl.ds(piece * half, half)],
+        lambda slot: r.mix_send.at[slot],
+        lambda slot: r.mix_recv.at[slot],
+    )
+
+    def across(k, q, whose):
+        ref = r.tok.at[2 * zsource(k) + whose, q]
+        return remote(ref, ref, r.pair_send.at[k, q], r.pair_recv.at[k, q], (partner, t))
+
+    def along(k):
+        to = 2 * lax.rem(z + nz - k, nz) + c
+        ref = r.tok.at[e, t]
+        return remote(ref, ref, r.z_send.at[k], r.z_recv.at[k], (to, t))
+
+    def along_in(k):
+        ref = r.tok.at[2 * zsource(k) + c, t]
+        return remote(ref, ref, r.z_send.at[k], r.z_recv.at[k], (e, t))
+
+    def route_to(by):
+        ref = r.route.at[e]
+        return remote(ref, ref, r.route_send.at[by], r.route_recv.at[e], (lax.rem(e + by, n_ep), t))
+
+    def route_from(source):
+        ref = r.route.at[source]
+        return remote(ref, ref, r.route_send.at[0], r.route_recv.at[source], (e, t))
+
+    edges = ((r.v_x, r.halo_x), (r.v_b, r.halo_b), (r.v_c, r.halo_c))
+
+    def halo(i):
+        src, dst = edges[i]
+        return remote(
+            src.at[pl.ds(rows - HALO, HALO)], dst, r.halo_send.at[i], r.halo_recv.at[i], (lax.rem(e + 1, n_ep), t)
+        )
+
+    got("rows", "scale")
+    step_rows = 16
+
+    def norm_rows(i, _):
+        part = r.v_rows[at(i * step_rows, step_rows), :].astype(f32)
+        by = lax.rsqrt(jnp.mean(part * part, axis=-1, keepdims=True) + epsilon)
+        part = (part * by * r.v_scale[...]).astype(bf16)
+        for q in range(tp):
+            r.tok[e, q, at(i * step_rows, step_rows), :] = part[:, q * quarter : (q + 1) * quarter]
+        return 0
+
+    lax.fori_loop(0, rows // step_rows, norm_rows, 0)
+    got("ids", "wts")
+    below = iota((rows, rows), 0)
+    right = iota((rows, rows), 1)
+    eye = (below == right).astype(f32)
+    r.earlier[...] = (below < right).astype(bf16)
+    r.route[e, 0:TOP_K, :] = dot(r.v_ids[...].astype(f32), eye, ((0,), (0,)), exact=True)
+    r.route[e, TOP_K : 2 * TOP_K, :] = dot(r.v_wts[...], eye, ((0,), (0,)), exact=True)
+    got("x", "b", "c")
+    pl.semaphore_wait(barrier, n_ep - 1 + 2)
+
+    @pl.when(e + 1 < n_ep)
+    def _():
+        for i in range(3):
+            halo(i).start()
+
+    for by in range(1, n_ep):
+        route_to(by).start()
+    for k in range(1, nz):
+        along(k).start()
+    for q in range(tp):
+        across(0, q, c).start()
+
+    @pl.when(e > 0)
+    def _():
+        for i in range(3):
+            halo(i).wait_recv()
+
+    @pl.when(e == 0)
+    def _():
+        for _, dst in edges:
+            dst[...] = jnp.zeros_like(dst)
+
+    got("vk", "bk", "ck", "step", "extra", "hld")
+
+    def conv(src, edge, taps, out):
+        def chunk(i, _):
+            lanes = at(i * LANES, LANES)
+            r.padded[0:8, :] = edge[:, lanes].astype(f32)[HALO - 8 :]
+            r.padded[8 : 8 + rows, :] = src[:, lanes].astype(f32)
+            total = jnp.zeros((rows, LANES), f32)
+            for k in range(CONV_TAPS):
+                lead = 8 - CONV_TAPS + 1 + k
+                total = total + r.padded[lead : lead + rows, :] * taps[k : k + 1, lanes]
+            out[:, lanes] = silu(total).astype(bf16)
+            return 0
+
+        lax.fori_loop(0, src.shape[1] // LANES, chunk, 0)
+
+    conv(r.v_x, r.halo_x, r.v_vk, r.vals)
+    conv(r.v_b, r.halo_b, r.v_bk, r.inm)
+    conv(r.v_c, r.halo_c, r.v_ck, r.outm)
+    pre = r.v_step[...]
+    steps = jnp.maximum(pre, 0.0) + jnp.log(1.0 + jnp.exp(-jnp.abs(pre)))
+    decay = -jnp.exp(r.v_hld[...]) * steps + r.v_extra[...]
+    upto = (below <= right).astype(f32)
+    cum = dot(upto, decay, ((0,), (0,)), exact=True)
+    r.cum[...] = cum
+    r.cum_t[...] = dot(decay, upto, ((0,), (0,)), exact=True)
+    r.step_t[...] = dot(steps, eye, ((0,), (0,)), exact=True)
+    spread_heads = (lax.div(iota((heads, width), 1), HEAD_DIM) == iota((heads, width), 0)).astype(f32)
+    r.growth[...] = dot(jnp.exp(cum), spread_heads, exact=True)
+    to_end = jnp.exp(cum[rows - 1 : rows, :] - cum) * steps
+    r.to_end[...] = dot(to_end, spread_heads, exact=True)
+    for g in range(groups):
+        lanes = pl.ds(g * band, band)
+        weighted = (r.vals[:, lanes].astype(f32) * r.to_end[:, lanes]).astype(bf16)
+        r.state[:, lanes] = dot(r.inm[:, g * STATE : (g + 1) * STATE], weighted, ((0,), (0,)))
+    r.state_out[...] = r.state[...].astype(bf16)
+    r.decay_out[...] = jnp.broadcast_to(r.growth[rows - 1 : rows, :], (8, width))
+
+    def swap(i):
+        src, dst = ((r.state_out, r.state_in), (r.decay_out, r.decay_in))[i]
+        return remote(src, dst, r.swap_send.at[i], r.swap_recv.at[i], (partner, t))
+
+    for i in range(2):
+        swap(i).start()
+    side = width // 2
+    mine_lanes = at(c * side, side)
+
+    def chain(i, by):
+        src, dst = ((r.chip_state, r.chain_state), (r.chip_decay, r.chain_decay))[i]
+        to = 2 * lax.rem(z + by, nz) + c
+        return remote(src, dst.at[z], r.chain_send.at[i, by], r.chain_recv.at[i, z], (to, t))
+
+    def chain_in(i, source):
+        src, dst = ((r.chip_state, r.chain_state), (r.chip_decay, r.chain_decay))[i]
+        return remote(src, dst.at[source], r.chain_send.at[i, 0], r.chain_recv.at[i, source], (e, t))
+
+    def send_chain():
+        for i in range(2):
+            swap(i).wait_recv()
+        ours, theirs = r.state[:, mine_lanes], r.state_in[:, mine_lanes].astype(f32)
+        our_decay, their_decay = r.decay_out[:, mine_lanes], r.decay_in[:, mine_lanes]
+        first = jnp.where(c == 0, ours, theirs)
+        second = jnp.where(c == 0, theirs, ours)
+        late = jnp.where(c == 0, their_decay, our_decay)
+        r.chip_state[...] = (late[0:1, :] * first + second).astype(bf16)
+        r.chip_decay[...] = our_decay * their_decay
+        for by in range(1, nz):
+
+            @pl.when(z + by < nz)
+            def _():
+                for i in range(2):
+                    chain(i, by).start()
+
+    def inside():
+        mid = rows // 2
+        lane = iota((mid, 2 * HEAD_DIM), 1) < HEAD_DIM
+        for g in range(groups):
+            cols = slice(g * STATE, (g + 1) * STATE)
+            for part in range(2):
+                span = slice(part * mid, (part + 1) * mid)
+                reach = (part + 1) * mid
+                scores = dot(r.outm[span, cols], r.inm[0:reach, cols], ((1,), (1,)))
+                mask = iota((mid, reach), 0) + part * mid >= iota((mid, reach), 1)
+                for p in range(ratio // 2):
+                    pair = []
+                    head = g * ratio + 2 * p
+                    lanes = slice(head * HEAD_DIM, (head + 2) * HEAD_DIM)
+                    for h in (head, head + 1):
+                        diff = r.cum[span, h : h + 1] - r.cum_t[h : h + 1, 0:reach]
+                        grid = scores * jnp.exp(jnp.where(mask, diff, -1e30)) * r.step_t[h : h + 1, 0:reach]
+                        pair.append(dot(grid.astype(bf16), r.vals[0:reach, lanes]))
+                    r.near[span, lanes] = jnp.where(lane, pair[0], pair[1])
+
+    def shared():
+        got("sg", "su")
+        gate, up = 0.0, 0.0
+        for q in range(tp):
+            part = r.tok[e, q]
+            gate = gate + dot(part, r.v_sg[q * quarter : (q + 1) * quarter, :])
+            up = up + dot(part, r.v_su[q * quarter : (q + 1) * quarter, :])
+        r.mix[t, :, width : width + sff] = (silu(gate) * up).astype(bf16)
+
+    def enter(k):
+        source = zsource(k)
+        seats = iota((cap, rows), 0).astype(f32)
+        for c2 in range(2):
+            block = 2 * source + c2
+            ids = r.route[block, 0:TOP_K, :]
+            weights = r.route[block, TOP_K : 2 * TOP_K, :]
+            for j in range(2):
+                hit = ids == (2 * e + j).astype(f32)
+                named = jnp.sum(jnp.where(hit, 1.0, 0.0), axis=0, keepdims=True)
+                given = jnp.sum(jnp.where(hit, weights, 0.0), axis=0, keepdims=True)
+                count = dot(jnp.broadcast_to(named, (16, rows)).astype(bf16), r.earlier[...])
+                seat = jnp.where(named > 0.0, count[0:1, :], -1.0)
+                taken = seats == seat
+                r.pick[k, c2, j * cap : (j + 1) * cap, :] = jnp.where(taken, 1.0, 0.0).astype(bf16)
+                amount = jnp.sum(jnp.where(taken, given, 0.0), axis=1, keepdims=True)
+                r.amount[k, j, c2 * cap : (c2 + 1) * cap, :] = jnp.broadcast_to(amount, (cap, LANES))
+            for q in range(tp):
+                chosen = dot(r.pick[k, c2], r.tok[block, q]).astype(bf16)
+                for j in range(2):
+                    r.arrived[j, c2 * cap : (c2 + 1) * cap, q * quarter : (q + 1) * quarter] = chosen[
+                        j * cap : (j + 1) * cap, :
+                    ]
+        for j in range(2):
+            gate = dot(r.arrived[j], r.v_wg[j])
+            up = dot(r.arrived[j], r.v_wu[j])
+            r.hid[k, t, j * 2 * cap : (j + 1) * 2 * cap, :] = (silu(gate) * up).astype(bf16)
+
+    def stage(k, _):
+        @pl.when(k > 0)
+        def _():
+            tokens(k).relay()
+
+        @pl.when(k + 1 < nz)
+        def _():
+            along_in(k + 1).wait_recv()
+            tokens(k + 1).start()
+            across(k + 1, t, c).start()
+
+        @pl.when(k == 0)
+        def _():
+            send_chain()
+            route_from(partner).wait_recv()
+            got("wg", "wu")
+
+        @pl.when(k == 1)
+        def _():
+            inside()
+
+        @pl.when(k == 2)
+        def _():
+            shared()
+
+        @pl.when(k > 0)
+        def _():
+            tokens(k).finish()
+            for q in (tx, ty, td):
+                across(k, q, c).start()
+            for c2 in range(2):
+                route_from(2 * zsource(k) + c2).wait_recv()
+
+        @pl.when(k > 1)
+        def _():
+            hiddens(k - 2).relay()
+
+        for q in range(tp):
+            across(k, q, other).wait_recv()
+        enter(k)
+        hiddens(k).start()
+        return 0
+
+    lax.fori_loop(0, nz, stage, 0)
+    hiddens(nz - 2).relay()
+
+    r.before[...] = jnp.zeros_like(r.before)
+
+    def add_chain(source, _):
+        @pl.when(source < z)
+        def _():
+            for i in range(2):
+                chain_in(i, source).wait_recv()
+            r.before[...] = r.chain_decay[source, 0:1, :] * r.before[...] + r.chain_state[source].astype(f32)
+
+        return 0
+
+    lax.fori_loop(0, nz, add_chain, 0)
+    r.incoming[c] = r.before[...].astype(bf16)
+
+    def halves(whose):
+        ref = r.incoming.at[whose]
+        return remote(ref, ref, r.half_sem.at[0], r.half_sem.at[1], (partner, t))
+
+    halves(c).start()
+    hiddens(nz - 1).relay()
+    got("wd", "gate", "skip", "mscale")
+
+    def back_pair(k):
+        return remote(r.yours.at[k], r.theirs.at[k], r.pair_y_send.at[k], r.pair_y_recv.at[k], (partner, t))
+
+    def back(k):
+        return remote(
+            r.going.at[k], r.coming.at[k], r.y_send.at[k], r.y_recv.at[k], (2 * zsource(k) + c, t)
+        )
+
+    def leave(k):
+        hiddens(k).finish()
+        for j in range(2):
+            total = 0.0
+            for q in range(tp):
+                total = total + dot(
+                    r.hid[k, q, j * 2 * cap : (j + 1) * 2 * cap, :], r.v_wd[j, q * ff : (q + 1) * ff, :]
+                )
+            total = (total * r.amount[k, j, :, 0:1]).astype(bf16)
+            for c2 in range(2):
+                r.result[c2, j * cap : (j + 1) * cap, :] = total[c2 * cap : (c2 + 1) * cap, :]
+        r.yours[k] = dot(r.pick[k, other], r.result[other], ((0,), (0,))).astype(bf16)
+        back_pair(k).start()
+        r.ours[k] = dot(r.pick[k, c], r.result[c], ((0,), (0,)))
+
+    def send_back(k):
+        back_pair(k).wait_recv()
+        r.going[k] = (r.ours[k] + r.theirs[k].astype(f32)).astype(bf16)
+        back(k).start()
+
+    def mixer_end():
+        halves(other).wait_recv()
+        spread_heads = (lax.div(iota((heads, width), 1), HEAD_DIM) == iota((heads, width), 0)).astype(f32)
+        skip = dot(jnp.broadcast_to(r.v_skip[...], (8, heads)), spread_heads, exact=True)[0:1, :]
+        for s in range(2):
+            lanes = slice(s * side, (s + 1) * side)
+            hold = r.incoming[s].astype(f32)
+            later = r.decay_in[0:1, lanes] * hold + r.state_in[:, lanes].astype(f32)
+            r.entering[:, lanes] = jnp.where(c == 0, hold, later).astype(bf16)
+        for g in range(groups):
+            lanes = slice(g * band, (g + 1) * band)
+            far = dot(r.outm[:, g * STATE : (g + 1) * STATE], r.entering[:, lanes]) * r.growth[:, lanes]
+            mixed = r.near[:, lanes] + far + skip[:, lanes] * r.vals[:, lanes].astype(f32)
+            gated = mixed * silu(r.v_gate[:, lanes].astype(f32))
+            by = lax.rsqrt(jnp.mean(gated * gated, axis=-1, keepdims=True) + epsilon)
+            r.mix[t, :, lanes] = (gated * by * r.v_mscale[:, lanes]).astype(bf16)
+
+    def leaving(i, _):
+        k = lax.rem(i + 1, nz)
+        leave(k)
+
+        @pl.when(i == 0)
+        def _():
+            mixer_end()
+            mixes.start()
+
+        @pl.when(i > 0)
+        def _():
+            send_back(i)
+
+        return 0
+
+    lax.fori_loop(0, nz, leaving, 0)
+    mixes.relay()
+    got("sd", "wm")
+
+    back_pair(0).wait_recv()
+    routed = r.ours[0] + r.theirs[0].astype(f32)
+    r.routed_sum[...] = routed + dot(r.mix[t, :, width : width + sff], r.v_sd[at(t * sff, sff), :])
+    r.mixer_sum[...] = dot(r.mix[t, :, 0:width], r.v_wm[at(t * width, width), :])
+    mixes.finish()
+    for q in (tx, ty, td):
+        r.routed_sum[...] += dot(r.mix[q, :, width : width + sff], r.v_sd[at(q * sff, sff), :])
+        r.mixer_sum[...] += dot(r.mix[q, :, 0:width], r.v_wm[at(q * width, width), :])
+    r.mixer_out[...] = r.mixer_sum[...].astype(bf16)
+    total = r.routed_sum[...]
+    for k in range(1, nz):
+        back(k).wait_recv()
+        total = total + r.coming[k].astype(f32)
+    r.routed_out[...] = total.astype(bf16)
+
+    @pl.when(e + 1 < n_ep)
+    def _():
+        for i in range(3):
+            halo(i).wait_send()
+
+    for by in range(1, n_ep):
+        route_to(by).wait_send()
+    for i in range(2):
+        swap(i).wait_send()
+    for by in range(1, nz):
+
+        @pl.when(z + by < nz)
+        def _():
+            for i in range(2):
+                chain(i, by).wait_send()
+
+    halves(c).wait_send()
+    mixes.drain()
+
+    def drain(k, _):
+        @pl.when(k > 0)
+        def _():
+            along(k).wait_send()
+            tokens(k).drain()
+            back(k).wait_send()
+
+        for q in range(tp):
+            across(k, q, c).wait_send()
+        hiddens(k).drain()
+        back_pair(k).wait_send()
+        return 0
+
+    lax.fori_loop(0, nz, drain, 0)
+
+
+def fused_on_device(*given):
+    argument = dict(zip(ARGUMENTS, given))
+    rows, model_width = argument["rows"].shape
+    n_ep, tp = lax.axis_size("ep"), lax.axis_size("tp")
+    nz = n_ep // 2
+    heads = argument["step"].shape[1]
+    width = argument["x"].shape[1]
+    state_width = argument["b"].shape[1]
+    groups = state_width // STATE
+    local_experts, _, ff = argument["wg"].shape
+    sff = argument["sg"].shape[1]
+    quarter = argument["wd"].shape[2]
+    cap = max(2, 3 * rows * TOP_K // (2 * local_experts * n_ep))
+    for name in ("hld", "skip", "mscale", "scale"):
+        argument[name] = argument[name].reshape(1, -1)
+    dims = types.SimpleNamespace(
+        n_ep=n_ep, tp=tp, rows=rows, cap=cap, ratio=heads // groups, quarter=quarter, heads=heads,
+        groups=groups, width=width, ff=ff, sff=sff,
+        fetched=FETCHED,
+    )
+    f32, bf16 = jnp.float32, jnp.bfloat16
+    scratch = dict(("v_" + n, pltpu.VMEM(argument[n].shape, argument[n].dtype)) for n in FETCHED)
+    vmem = dict(
+        tok=((n_ep, tp, rows, quarter), bf16),
+        hid=((nz, tp, 4 * cap, ff), bf16),
+        mix=((tp, rows, width + sff), bf16),
+        route=((n_ep, 2 * TOP_K, rows), f32),
+        halo_x=((HALO, width), bf16),
+        halo_b=((HALO, state_width), bf16),
+        halo_c=((HALO, state_width), bf16),
+        padded=((8 + rows, LANES), f32),
+        vals=((rows, width), bf16),
+        inm=((rows, state_width), bf16),
+        outm=((rows, state_width), bf16),
+        cum=((rows, heads), f32),
+        cum_t=((heads, rows), f32),
+        step_t=((heads, rows), f32),
+        growth=((rows, width), f32),
+        to_end=((rows, width), f32),
+        state=((STATE, width), f32),
+        state_out=((STATE, width), bf16),
+        state_in=((STATE, width), bf16),
+        decay_out=((8, width), f32),
+        decay_in=((8, width), f32),
+        chip_state=((STATE, width // 2), bf16),
+        chip_decay=((8, width // 2), f32),
+        chain_state=((nz, STATE, width // 2), bf16),
+        chain_decay=((nz, 8, width // 2), f32),
+        before=((STATE, width // 2), f32),
+        incoming=((2, STATE, width // 2), bf16),
+        entering=((STATE, width), bf16),
+        near=((rows, width), f32),
+        earlier=((rows, rows), bf16),
+        pick=((nz, 2, 2 * cap, rows), bf16),
+        amount=((nz, 2, 2 * cap, LANES), f32),
+        arrived=((2, 2 * cap, model_width), bf16),
+        result=((2, 2 * cap, quarter), bf16),
+        yours=((nz, rows, quarter), bf16),
+        theirs=((nz, rows, quarter), bf16),
+        ours=((nz, rows, quarter), f32),
+        going=((nz, rows, quarter), bf16),
+        coming=((nz, rows, quarter), bf16),
+        routed_sum=((rows, quarter), f32),
+        mixer_sum=((rows, quarter), f32),
+    )
+    for name, (shape, dtype) in vmem.items():
+        scratch[name] = pltpu.VMEM(shape, dtype)
+    sems = dict(
+        local_sem=(len(FETCHED),),
+        tok_send=(nz, 6), tok_recv=(nz, 6), hid_send=(nz, 6), hid_recv=(nz, 6),
+        mix_send=(6,), mix_recv=(6,), pair_send=(nz, tp), pair_recv=(nz, tp),
+        z_send=(nz,), z_recv=(nz,), route_send=(n_ep,), route_recv=(n_ep,),
+        halo_send=(3,), halo_recv=(3,), swap_send=(2,), swap_recv=(2,),
+        chain_send=(2, nz), chain_recv=(2, nz), half_sem=(2,),
+        pair_y_send=(nz,), pair_y_recv=(nz,), y_send=(nz,), y_recv=(nz,),
+    )
+    for name, shape in sems.items():
+        scratch[name] = pltpu.SemaphoreType.DMA(shape)
+    order = tuple(FETCHED)
+    names = order + ("mixer_out", "routed_out") + tuple(scratch)
+    out = jax.ShapeDtypeStruct((rows, quarter), bf16)
+    return tuple(
+        pl.pallas_call(
+            functools.partial(body, dims, names),
+            out_shape=(out, out),
+            in_specs=[pl.BlockSpec(memory_space=pl.ANY)] * len(order),
+            out_specs=(pl.BlockSpec(memory_space=pltpu.VMEM),) * 2,
+            scratch_shapes=list(scratch.values()),
+            compiler_params=pltpu.CompilerParams(
+                collective_id=0, has_side_effects=True, vmem_limit_bytes=VMEM_LIMIT
+            ),
+            name="mixer_and_experts",
+        )(*[argument[n] for n in order])
+    )
+
+
+VMEM_LIMIT = 60 * 1024 * 1024
+ARGUMENTS = (
+    "x", "b", "c", "gate", "step", "extra", "hld", "skip", "vk", "bk", "ck", "mscale", "wm",
+    "rows", "scale", "ids", "wts", "wg", "wu", "wd", "sg", "su", "sd",
+)
+FETCHED = (
+    "rows", "scale", "ids", "wts", "x", "b", "c", "vk", "bk", "ck", "step", "extra", "hld",
+    "wg", "wu", "sg", "su", "gate", "skip", "mscale", "wd", "sd", "wm",
+)
+
+
+def choose(*given):
+    argument = dict(zip(ARGUMENTS, given))
+    n_ep, tp = lax.axis_size("ep"), lax.axis_size("tp")
+    rows = argument["rows"].shape[0]
+    experts = argument["wg"].shape[0]
+    cap = max(2, 3 * rows * TOP_K // (2 * experts * n_ep))
+    wide = all(argument[n].shape[-1] % LANES == 0 for n in ("x", "b", "wg", "wd", "sg"))
+    fits = tp == 4 and n_ep % 2 == 0 and n_ep >= 6 and experts == 2
+    fits = fits and wide and cap % 16 == 0 and rows % 32 == 0
+    return fused_on_device(*given) if fits else on_device(*given)
+
+
 def solution(mesh):
     return jax.shard_map(
-        on_device,
+        choose,
         mesh=mesh,
         in_specs=(
             P("ep", "tp"),

time: 241 us -> 111 us (0.46)
  Pallas kernels: 0 us -> 101 us
  waiting for transfers between devices: 87.8 us -> 0 us
  matrix products: 37.4 us -> 0 us
  starting transfers between devices: 36.9 us -> 0 us
  other arithmetic: 28.6 us -> 0 us
  local copies, waits for them, and re-layouts: 34.6 us -> 9.24 us
  between operations: 14.4 us -> 0.64 us
    pallas_call x0 -> x1, Pallas kernels: none -> 101 us  [fused_on_device(): pl.pallas_call(functools.partial(body, dims, names), out_shape=(out, out)...]
    all_gather x4 -> x0, waiting for transfers between devices: 77.5 us -> none  [the longest x1 31.1 us: on_device(): column_piece = lax.all_gather(arrived, 'tp', axis=2, tiled=True)]
    dot_general x17 -> x0, matrix products: 37.4 us -> none  [the longest x1 5.34 us: on_device(): jnp.einsum('esd,edf->esf', column_piece, routed_gate_weight, preferred_el...]
    ppermute x8 -> x0, starting transfers between devices: 32 us -> none  [passed_along(): return lax.ppermute(x, axis, pairs)]
    slice x15 -> x0, local copies, waits for them, and re-layouts: 10.2 us -> none  [the longest x1 1.88 us: on_device(): whole_mix = both[:, :, :width_x].reshape(length, -1)]
    convert_element_type x11 -> x0, other arithmetic: 9.61 us -> none  [the longest x1 3.43 us: conv_silu(): return jax.nn.silu(total_sum).astype(jnp.bfloat16)]
    ppermute x8 -> x0, waiting for transfers between devices: 9.39 us -> none  [passed_along(): return lax.ppermute(x, axis, pairs)]
    reshape x6 -> x0, local copies, waits for them, and re-layouts: 8.05 us -> none  [the longest x1 3.15 us: on_device(): mixed_heads = (inside + carried_term).reshape(length, heads_local, HEAD_DIM)]
  transfers between devices with their start and end apart: 13 -> 0, of which waited for: 10 -> 0; matrix products, arithmetic and copies ran while one was open for 30% -> 0% of each run, Pallas kernels for 0% -> 0%
where the time goes in v1:
time: 111 us
  Pallas kernels  101 us (91%)
  local copies, waits for them, and re-layouts  9.24 us (8%)
    pallas_call x1, Pallas kernels, fused_on_device(): pl.pallas_call(functools.partial(body, dims, names), out_shape=(out, out)...  101 us
    unnamed x6, local copies, waits for them, and re-layouts  9.24 us

profile of v1, /device:TPU:0, one launch (start us, length us, event | category | flops | bytes accessed | tf_op | source)
XLA Modules:
  0.0 110.9 jit_solution(16838975943727459570)
XLA Ops:
  0.6 1.5 %copy.27.refs_10_ = f32[256,16]{1,0:T(8,128)} copy(f32[256,16]{0,1:T(8,128)} %param.27) | data formatting | bytes 32768 | tf_op args[4]
  2.1 1.5 %copy.28.refs_11_ = f32[256,16]{1,0:T(8,128)} copy(f32[256,16]{0,1:T(8,128)} %param.28) | data formatting | bytes 32768 | tf_op args[5]
  3.6 1.5 %copy.25.refs_2_ = s32[256,4]{1,0:T(8,128)} copy(s32[256,4]{0,1:T(4,128)} %param.38) | data formatting | bytes 8192 | tf_op args[15]
  5.0 1.5 %copy.26.refs_3_ = f32[256,4]{1,0:T(8,128)} copy(f32[256,4]{0,1:T(4,128)} %param.39) | data formatting | bytes 8192 | tf_op args[16]
  6.5 101.0 %mixer_and_experts.1 = (bf16[256,512]{1,0:T(8,128)(2,1)}, bf16[256,512]{1,0:T(8,128)(2,1)}) custom-call(bf16[256,2048]{1,0:T(8,128)(2,1)} %refs_0_.1, f32[1,2048]{1,0:T(1,128)} %bitcast.4, s32[256,4]{1,0:T(8,128)} %copy.25.refs_2_, f32[256,4]{1,0:T(8,128)} %copy.26.refs_3_, bf16[256,1024]{1,0:T(8,128)(2,1)} %refs_4_.1, bf16[256,512]{1,0:T(8,128)(2,1)} %refs_5_.1, ...), custom_call_target="tpu_custom_call" | custom-call | tf_op jit(solution)/shard_map/mixer_and_experts/pallas_call | solution.py:855
  107.5 1.7 %copy.31 = bf16[256,512]{1,0:T(8,128)(2,1)} copy(bf16[256,512]{1,0:T(8,128)(2,1)} %get-tuple-element.4) | data formatting | bytes 524288
  109.2 1.7 %copy.32 = bf16[256,512]{1,0:T(8,128)(2,1)} copy(bf16[256,512]{1,0:T(8,128)(2,1)} %get-tuple-element.5) | data formatting | bytes 524288

commit v2 on v1

--- a/solution.py
+++ b/solution.py
@@ -329,8 +329,13 @@
     for to in (tx, ty):
         pl.semaphore_signal(barrier, inc=1, device_id=(e, to), device_id_type=MESH)
 
+    paired = jnp.minimum(z, nz - 1 - z)
+
     def zsource(k):
-        return lax.rem(z + k, nz)
+        inward = jnp.where(2 * z > nz - 1, -1, 1)
+        alternate = z + inward * lax.div(k + 1, 2) * (2 * lax.rem(k, 2) - 1)
+        rest = z + inward * (k - paired)
+        return jnp.where(k <= 2 * paired, alternate, rest)
 
     def plane(buf, send, recv):
         def leg(q, piece, slot, to):
@@ -348,11 +353,12 @@
             leg(ty, 1, 3, ty).wait_recv()
             leg(ty, 1, 5, tx).start()
 
+        def rest():
+            return leg(tx, 1, 1, tx), leg(ty, 0, 2, ty), leg(td, 0, 4, ty), leg(td, 1, 5, tx)
+
         def finish():
-            leg(tx, 1, 1, tx).wait_recv()
-            leg(ty, 0, 2, ty).wait_recv()
-            leg(td, 0, 4, ty).wait_recv()
-            leg(td, 1, 5, tx).wait_recv()
+            for one in rest():
+                one.wait_recv()
 
         def drain():
             leg(t, 0, 0, tx).wait_send()
@@ -362,15 +368,14 @@
             leg(tx, 0, 4, ty).wait_send()
             leg(ty, 1, 5, tx).wait_send()
 
-        return types.SimpleNamespace(start=start, relay=relay, finish=finish, drain=drain)
-
-    def tokens(k):
-        block = 2 * zsource(k) + c
-        return plane(
-            lambda q, piece: r.tok.at[block, q, pl.ds(piece * half, half)],
-            lambda slot: r.tok_send.at[k, slot],
-            lambda slot: r.tok_recv.at[k, slot],
-        )
+        return types.SimpleNamespace(start=start, relay=relay, rest=rest, finish=finish, drain=drain)
+
+    def token_leg(source, q, piece, slot, to):
+        ref = r.tok.at[2 * source + c, q, pl.ds(piece * half, half)]
+        return remote(ref, ref, r.tok_send.at[source, slot], r.tok_recv.at[source, slot], (e, to))
+
+    def token_legs(source, piece):
+        return token_leg(source, t, piece, piece, tx), token_leg(source, t, piece, 2 + piece, ty)
 
     def hiddens(k):
         return plane(
@@ -379,24 +384,63 @@
             lambda slot: r.hid_recv.at[k, slot],
         )
 
+    shares = plane(
+        lambda q, piece: r.share.at[q, pl.ds(piece * half, half)],
+        lambda slot: r.share_send.at[slot],
+        lambda slot: r.share_recv.at[slot],
+    )
     mixes = plane(
         lambda q, piece: r.mix.at[q, pl.ds(piece * half, half)],
         lambda slot: r.mix_send.at[slot],
         lambda slot: r.mix_recv.at[slot],
     )
 
-    def across(k, q, whose):
-        ref = r.tok.at[2 * zsource(k) + whose, q]
-        return remote(ref, ref, r.pair_send.at[k, q], r.pair_recv.at[k, q], (partner, t))
-
-    def along(k):
-        to = 2 * lax.rem(z + nz - k, nz) + c
-        ref = r.tok.at[e, t]
-        return remote(ref, ref, r.z_send.at[k], r.z_recv.at[k], (to, t))
-
-    def along_in(k):
-        ref = r.tok.at[2 * zsource(k) + c, t]
-        return remote(ref, ref, r.z_send.at[k], r.z_recv.at[k], (e, t))
+    def across(source, q, whose):
+        ref = r.tok.at[2 * source + whose, q]
+        return remote(ref, ref, r.pair_send.at[source, q], r.pair_recv.at[source, q], (partner, t))
+
+    def along(source, slot, up):
+        block = 2 * source + c
+        ref = r.tok.at[block, td] if slot == 2 else r.tok.at[block, t, pl.ds(slot * half, half)]
+        to = 2 * (z - 1 + 2 * up) + c
+        return remote(ref, ref, r.z_send.at[source, slot, up], r.z_recv.at[source, slot], (to, t))
+
+    def onward(up):
+        return z + 1 < nz if up else z - 1 >= 0
+
+    def sides(s, act):
+        @pl.when(z - s >= 0)
+        def _():
+            act(z - s, 1)
+
+        @pl.when(z + s < nz)
+        def _():
+            act(z + s, 0)
+
+    def pass_on(source, slot, up):
+        along(source, slot, 1 - up).wait_recv()
+
+        @pl.when(onward(up))
+        def _():
+            along(source, slot, up).start()
+
+    def near_piece(piece, source, up):
+        pass_on(source, piece, up)
+        for one in token_legs(source, piece):
+            one.start()
+
+    def near_part(source, up):
+        near_piece(0, source, up)
+        near_piece(1, source, up)
+        across(source, t, c).start()
+
+    def near_rest(source, up):
+        near_piece(1, source, up)
+        across(source, t, c).start()
+
+    def far_part(source, up):
+        pass_on(source, 2, up)
+        across(source, td, c).start()
 
     def route_to(by):
         ref = r.route.at[e]
@@ -425,14 +469,13 @@
             r.tok[e, q, at(i * step_rows, step_rows), :] = part[:, q * quarter : (q + 1) * quarter]
         return 0
 
-    lax.fori_loop(0, rows // step_rows, norm_rows, 0)
+    lax.fori_loop(0, rows // step_rows, norm_rows, 0, unroll=4)
     got("ids", "wts")
     below = iota((rows, rows), 0)
     right = iota((rows, rows), 1)
-    eye = (below == right).astype(f32)
     r.earlier[...] = (below < right).astype(bf16)
-    r.route[e, 0:TOP_K, :] = dot(r.v_ids[...].astype(f32), eye, ((0,), (0,)), exact=True)
-    r.route[e, TOP_K : 2 * TOP_K, :] = dot(r.v_wts[...], eye, ((0,), (0,)), exact=True)
+    r.route[e, 0:TOP_K, :] = r.v_ids[...].astype(f32)
+    r.route[e, TOP_K : 2 * TOP_K, :] = r.v_wts[...]
     got("x", "b", "c")
     pl.semaphore_wait(barrier, n_ep - 1 + 2)
 
@@ -443,122 +486,23 @@
 
     for by in range(1, n_ep):
         route_to(by).start()
-    for k in range(1, nz):
-        along(k).start()
+    for slot in range(3):
+        for up in (1, 0):
+
+            @pl.when(onward(up))
+            def _():
+                along(z, slot, up).start()
+
     for q in range(tp):
-        across(0, q, c).start()
-
-    @pl.when(e > 0)
-    def _():
-        for i in range(3):
-            halo(i).wait_recv()
-
-    @pl.when(e == 0)
-    def _():
-        for _, dst in edges:
-            dst[...] = jnp.zeros_like(dst)
-
-    got("vk", "bk", "ck", "step", "extra", "hld")
-
-    def conv(src, edge, taps, out):
-        def chunk(i, _):
-            lanes = at(i * LANES, LANES)
-            r.padded[0:8, :] = edge[:, lanes].astype(f32)[HALO - 8 :]
-            r.padded[8 : 8 + rows, :] = src[:, lanes].astype(f32)
-            total = jnp.zeros((rows, LANES), f32)
-            for k in range(CONV_TAPS):
-                lead = 8 - CONV_TAPS + 1 + k
-                total = total + r.padded[lead : lead + rows, :] * taps[k : k + 1, lanes]
-            out[:, lanes] = silu(total).astype(bf16)
-            return 0
-
-        lax.fori_loop(0, src.shape[1] // LANES, chunk, 0)
-
-    conv(r.v_x, r.halo_x, r.v_vk, r.vals)
-    conv(r.v_b, r.halo_b, r.v_bk, r.inm)
-    conv(r.v_c, r.halo_c, r.v_ck, r.outm)
-    pre = r.v_step[...]
-    steps = jnp.maximum(pre, 0.0) + jnp.log(1.0 + jnp.exp(-jnp.abs(pre)))
-    decay = -jnp.exp(r.v_hld[...]) * steps + r.v_extra[...]
-    upto = (below <= right).astype(f32)
-    cum = dot(upto, decay, ((0,), (0,)), exact=True)
-    r.cum[...] = cum
-    r.cum_t[...] = dot(decay, upto, ((0,), (0,)), exact=True)
-    r.step_t[...] = dot(steps, eye, ((0,), (0,)), exact=True)
-    spread_heads = (lax.div(iota((heads, width), 1), HEAD_DIM) == iota((heads, width), 0)).astype(f32)
-    r.growth[...] = dot(jnp.exp(cum), spread_heads, exact=True)
-    to_end = jnp.exp(cum[rows - 1 : rows, :] - cum) * steps
-    r.to_end[...] = dot(to_end, spread_heads, exact=True)
-    for g in range(groups):
-        lanes = pl.ds(g * band, band)
-        weighted = (r.vals[:, lanes].astype(f32) * r.to_end[:, lanes]).astype(bf16)
-        r.state[:, lanes] = dot(r.inm[:, g * STATE : (g + 1) * STATE], weighted, ((0,), (0,)))
-    r.state_out[...] = r.state[...].astype(bf16)
-    r.decay_out[...] = jnp.broadcast_to(r.growth[rows - 1 : rows, :], (8, width))
-
-    def swap(i):
-        src, dst = ((r.state_out, r.state_in), (r.decay_out, r.decay_in))[i]
-        return remote(src, dst, r.swap_send.at[i], r.swap_recv.at[i], (partner, t))
-
-    for i in range(2):
-        swap(i).start()
-    side = width // 2
-    mine_lanes = at(c * side, side)
-
-    def chain(i, by):
-        src, dst = ((r.chip_state, r.chain_state), (r.chip_decay, r.chain_decay))[i]
-        to = 2 * lax.rem(z + by, nz) + c
-        return remote(src, dst.at[z], r.chain_send.at[i, by], r.chain_recv.at[i, z], (to, t))
-
-    def chain_in(i, source):
-        src, dst = ((r.chip_state, r.chain_state), (r.chip_decay, r.chain_decay))[i]
-        return remote(src, dst.at[source], r.chain_send.at[i, 0], r.chain_recv.at[i, source], (e, t))
-
-    def send_chain():
-        for i in range(2):
-            swap(i).wait_recv()
-        ours, theirs = r.state[:, mine_lanes], r.state_in[:, mine_lanes].astype(f32)
-        our_decay, their_decay = r.decay_out[:, mine_lanes], r.decay_in[:, mine_lanes]
-        first = jnp.where(c == 0, ours, theirs)
-        second = jnp.where(c == 0, theirs, ours)
-        late = jnp.where(c == 0, their_decay, our_decay)
-        r.chip_state[...] = (late[0:1, :] * first + second).astype(bf16)
-        r.chip_decay[...] = our_decay * their_decay
-        for by in range(1, nz):
-
-            @pl.when(z + by < nz)
-            def _():
-                for i in range(2):
-                    chain(i, by).start()
-
-    def inside():
-        mid = rows // 2
-        lane = iota((mid, 2 * HEAD_DIM), 1) < HEAD_DIM
-        for g in range(groups):
-            cols = slice(g * STATE, (g + 1) * STATE)
-            for part in range(2):
-                span = slice(part * mid, (part + 1) * mid)
-                reach = (part + 1) * mid
-                scores = dot(r.outm[span, cols], r.inm[0:reach, cols], ((1,), (1,)))
-                mask = iota((mid, reach), 0) + part * mid >= iota((mid, reach), 1)
-                for p in range(ratio // 2):
-                    pair = []
-                    head = g * ratio + 2 * p
-                    lanes = slice(head * HEAD_DIM, (head + 2) * HEAD_DIM)
-                    for h in (head, head + 1):
-                        diff = r.cum[span, h : h + 1] - r.cum_t[h : h + 1, 0:reach]
-                        grid = scores * jnp.exp(jnp.where(mask, diff, -1e30)) * r.step_t[h : h + 1, 0:reach]
-                        pair.append(dot(grid.astype(bf16), r.vals[0:reach, lanes]))
-                    r.near[span, lanes] = jnp.where(lane, pair[0], pair[1])
-
-    def shared():
-        got("sg", "su")
-        gate, up = 0.0, 0.0
-        for q in range(tp):
-            part = r.tok[e, q]
-            gate = gate + dot(part, r.v_sg[q * quarter : (q + 1) * quarter, :])
-            up = up + dot(part, r.v_su[q * quarter : (q + 1) * quarter, :])
-        r.mix[t, :, width : width + sff] = (silu(gate) * up).astype(bf16)
+        across(z, q, c).start()
+    got("sg", "su")
+    gate, up = 0.0, 0.0
+    for q in range(tp):
+        part = r.tok[e, q]
+        gate = gate + dot(part, r.v_sg[q * quarter : (q + 1) * quarter, :])
+        up = up + dot(part, r.v_su[q * quarter : (q + 1) * quarter, :])
+    r.share[t] = (silu(gate) * up).astype(bf16)
+    shares.start()
 
     def enter(k):
         source = zsource(k)
@@ -588,83 +532,131 @@
             up = dot(r.arrived[j], r.v_wu[j])
             r.hid[k, t, j * 2 * cap : (j + 1) * 2 * cap, :] = (silu(gate) * up).astype(bf16)
 
-    def stage(k, _):
-        @pl.when(k > 0)
-        def _():
-            tokens(k).relay()
-
-        @pl.when(k + 1 < nz)
-        def _():
-            along_in(k + 1).wait_recv()
-            tokens(k + 1).start()
-            across(k + 1, t, c).start()
-
-        @pl.when(k == 0)
-        def _():
-            send_chain()
-            route_from(partner).wait_recv()
-            got("wg", "wu")
-
-        @pl.when(k == 1)
-        def _():
-            inside()
-
-        @pl.when(k == 2)
-        def _():
-            shared()
-
-        @pl.when(k > 0)
-        def _():
-            tokens(k).finish()
-            for q in (tx, ty, td):
-                across(k, q, c).start()
-            for c2 in range(2):
-                route_from(2 * zsource(k) + c2).wait_recv()
-
-        @pl.when(k > 1)
-        def _():
-            hiddens(k - 2).relay()
-
-        for q in range(tp):
-            across(k, q, other).wait_recv()
-        enter(k)
-        hiddens(k).start()
-        return 0
-
-    lax.fori_loop(0, nz, stage, 0)
-    hiddens(nz - 2).relay()
-
-    r.before[...] = jnp.zeros_like(r.before)
-
-    def add_chain(source, _):
-        @pl.when(source < z)
-        def _():
-            for i in range(2):
-                chain_in(i, source).wait_recv()
-            r.before[...] = r.chain_decay[source, 0:1, :] * r.before[...] + r.chain_state[source].astype(f32)
-
-        return 0
-
-    lax.fori_loop(0, nz, add_chain, 0)
-    r.incoming[c] = r.before[...].astype(bf16)
-
-    def halves(whose):
-        ref = r.incoming.at[whose]
-        return remote(ref, ref, r.half_sem.at[0], r.half_sem.at[1], (partner, t))
-
-    halves(c).start()
-    hiddens(nz - 1).relay()
-    got("wd", "gate", "skip", "mscale")
+    @pl.when(e > 0)
+    def _():
+        for i in range(3):
+            halo(i).wait_recv()
+
+    @pl.when(e == 0)
+    def _():
+        for _, dst in edges:
+            dst[...] = jnp.zeros_like(dst)
+
+    got("vk", "bk", "ck", "step", "extra", "hld")
+
+    def conv(src, edge, taps, out):
+        def chunk(i, _):
+            lanes = at(i * LANES, LANES)
+            r.padded[0:8, :] = edge[:, lanes].astype(f32)[HALO - 8 :]
+            r.padded[8 : 8 + rows, :] = src[:, lanes].astype(f32)
+            total = jnp.zeros((rows, LANES), f32)
+            for k in range(CONV_TAPS):
+                lead = 8 - CONV_TAPS + 1 + k
+                total = total + r.padded[lead : lead + rows, :] * taps[k : k + 1, lanes]
+            out[:, lanes] = silu(total).astype(bf16)
+            return 0
+
+        lax.fori_loop(0, src.shape[1] // LANES, chunk, 0)
+
+    conv(r.v_x, r.halo_x, r.v_vk, r.vals)
+    conv(r.v_b, r.halo_b, r.v_bk, r.inm)
+    conv(r.v_c, r.halo_c, r.v_ck, r.outm)
+    route_from(partner).wait_recv()
+    got("wg", "wu")
+    for q in range(tp):
+        across(z, q, other).wait_recv()
+    enter(0)
+    hiddens(0).start()
+    shares.relay()
+    sides(1, functools.partial(near_piece, 0))
+    pre = r.v_step[...]
+    steps = jnp.maximum(pre, 0.0) + jnp.log(1.0 + jnp.exp(-jnp.abs(pre)))
+    diagonal = iota((heads, heads), 0) == iota((heads, heads), 1)
+    rate = jnp.sum(jnp.where(diagonal, jnp.exp(r.v_hld[...]), 0.0), axis=1, keepdims=True)
+    decay = -rate * steps + r.v_extra[...]
+    upto = (below <= right).astype(f32)
+    cum_t = dot(decay, upto, exact=True)
+    cum = dot((right <= below).astype(f32), decay, ((1,), (1,)), exact=True)
+    r.cum[...] = cum
+    r.cum_t[...] = cum_t
+    r.step_t[...] = steps
+    spread_heads = (lax.div(iota((heads, width), 1), HEAD_DIM) == iota((heads, width), 0)).astype(f32)
+    r.growth[...] = dot(jnp.exp(cum), spread_heads, exact=True)
+    to_end = jnp.exp(cum_t[:, rows - 1 : rows] - cum_t) * steps
+    r.to_end[...] = dot(to_end, spread_heads, ((0,), (0,)), exact=True)
+    for g in range(groups):
+        lanes = pl.ds(g * band, band)
+        weighted = (r.vals[:, lanes].astype(f32) * r.to_end[:, lanes]).astype(bf16)
+        r.state[:, lanes] = dot(r.inm[:, g * STATE : (g + 1) * STATE], weighted, ((0,), (0,)))
+    r.state_out[...] = r.state[...].astype(bf16)
+    r.decay_out[...] = jnp.broadcast_to(r.growth[rows - 1 : rows, :], (8, width))
+
+    def swap(i):
+        src, dst = ((r.state_out, r.state_in), (r.decay_out, r.decay_in))[i]
+        return remote(src, dst, r.swap_send.at[i], r.swap_recv.at[i], (partner, t))
+
+    for i in range(2):
+        swap(i).start()
+    side = width // 2
+    mine_lanes = at(c * side, side)
+
+    def chain(i, by):
+        src, dst = ((r.chip_state, r.chain_state), (r.chip_decay, r.chain_decay))[i]
+        to = 2 * lax.rem(z + by, nz) + c
+        return remote(src, dst.at[z], r.chain_send.at[i, by], r.chain_recv.at[i, z], (to, t))
+
+    def chain_in(i, source):
+        src, dst = ((r.chip_state, r.chain_state), (r.chip_decay, r.chain_decay))[i]
+        return remote(src, dst.at[source], r.chain_send.at[i, 0], r.chain_recv.at[i, source], (e, t))
+
+    def send_chain():
+        for i in range(2):
+            swap(i).wait_recv()
+        ours, theirs = r.state[:, mine_lanes], r.state_in[:, mine_lanes].astype(f32)
+        our_decay, their_decay = r.decay_out[:, mine_lanes], r.decay_in[:, mine_lanes]
+        first = jnp.where(c == 0, ours, theirs)
+        second = jnp.where(c == 0, theirs, ours)
+        late = jnp.where(c == 0, their_decay, our_decay)
+        r.chip_state[...] = (late[0:1, :] * first + second).astype(bf16)
+        r.chip_decay[...] = our_decay * their_decay
+        for by in range(1, nz):
+
+            @pl.when(z + by < nz)
+            def _():
+                for i in range(2):
+                    chain(i, by).start()
+
+    def inside():
+        mid = rows // 2
+        lane = iota((mid, 2 * HEAD_DIM), 1) < HEAD_DIM
+        for g in range(groups):
+            cols = slice(g * STATE, (g + 1) * STATE)
+            for part in range(2):
+                span = slice(part * mid, (part + 1) * mid)
+                reach = (part + 1) * mid
+                scores = dot(r.outm[span, cols], r.inm[0:reach, cols], ((1,), (1,)))
+                mask = iota((mid, reach), 0) + part * mid >= iota((mid, reach), 1)
+                for p in range(ratio // 2):
+                    pair = []
+                    head = g * ratio + 2 * p
+                    lanes = slice(head * HEAD_DIM, (head + 2) * HEAD_DIM)
+                    for h in (head, head + 1):
+                        diff = r.cum[span, h : h + 1] - r.cum_t[h : h + 1, 0:reach]
+                        grid = scores * jnp.exp(jnp.where(mask, diff, -1e30)) * r.step_t[h : h + 1, 0:reach]
+                        pair.append(dot(grid.astype(bf16), r.vals[0:reach, lanes]))
+                    r.near[span, lanes] = jnp.where(lane, pair[0], pair[1])
 
     def back_pair(k):
         return remote(r.yours.at[k], r.theirs.at[k], r.pair_y_send.at[k], r.pair_y_recv.at[k], (partner, t))
 
     def back(k):
-        return remote(
-            r.going.at[k], r.coming.at[k], r.y_send.at[k], r.y_recv.at[k], (2 * zsource(k) + c, t)
-        )
-
-    def leave(k):
+        source = zsource(k)
+        return remote(r.going.at[k], r.coming.at[z], r.y_send.at[k], r.y_recv.at[z], (2 * source + c, t))
+
+    def back_in(source):
+        return remote(r.going.at[0], r.coming.at[source], r.y_send.at[0], r.y_recv.at[source], (e, t))
+
+    def leave(k, carry=0):
         hiddens(k).finish()
         for j in range(2):
             total = 0.0
@@ -678,11 +670,80 @@
         r.yours[k] = dot(r.pick[k, other], r.result[other], ((0,), (0,))).astype(bf16)
         back_pair(k).start()
         r.ours[k] = dot(r.pick[k, c], r.result[c], ((0,), (0,)))
-
-    def send_back(k):
+        return carry
+
+    def send_back(k, carry=0):
         back_pair(k).wait_recv()
         r.going[k] = (r.ours[k] + r.theirs[k].astype(f32)).astype(bf16)
         back(k).start()
+        return carry
+
+    sides(1, near_rest)
+    hiddens(0).relay()
+
+    def stage(k, _):
+        source = zsource(k)
+
+        sides(k, far_part)
+
+        @pl.when(k == 1)
+        def _():
+            inside()
+
+        @pl.when(k == 2)
+        def _():
+            got("wd")
+
+        @pl.when(k == nz - 1)
+        def _():
+            send_chain()
+
+        for piece in range(2):
+            token_leg(source, tx, piece, piece, tx).wait_recv()
+        across(source, tx, c).start()
+        for piece in range(2):
+            token_leg(source, ty, piece, 2 + piece, ty).wait_recv()
+        across(source, ty, c).start()
+        for c2 in range(2):
+            route_from(2 * source + c2).wait_recv()
+
+        sides(k + 1, near_part)
+        for q in range(tp):
+            across(source, q, other).wait_recv()
+        enter(k)
+
+        @pl.when(jnp.logical_and(k > 1, k < nz - 1))
+        def _():
+            hiddens(k - 1).relay()
+
+        hiddens(k).start()
+        return 0
+
+    lax.fori_loop(1, nz, stage, 0)
+    lax.fori_loop(1, nz - 2, leave, 0)
+    hiddens(nz - 2).relay()
+    lax.fori_loop(1, nz - 2, send_back, 0)
+
+    r.before[...] = jnp.zeros_like(r.before)
+
+    def add_chain(source, _):
+        @pl.when(source < z)
+        def _():
+            for i in range(2):
+                chain_in(i, source).wait_recv()
+            r.before[...] = r.chain_decay[source, 0:1, :] * r.before[...] + r.chain_state[source].astype(f32)
+
+        return 0
+
+    lax.fori_loop(0, nz, add_chain, 0)
+    r.incoming[c] = r.before[...].astype(bf16)
+
+    def halves(whose):
+        ref = r.incoming.at[whose]
+        return remote(ref, ref, r.half_sem.at[0], r.half_sem.at[1], (partner, t))
+
+    halves(c).start()
+    got("gate", "skip", "mscale")
 
     def mixer_end():
         halves(other).wait_recv()
@@ -701,39 +762,50 @@
             by = lax.rsqrt(jnp.mean(gated * gated, axis=-1, keepdims=True) + epsilon)
             r.mix[t, :, lanes] = (gated * by * r.v_mscale[:, lanes]).astype(bf16)
 
-    def leaving(i, _):
-        k = lax.rem(i + 1, nz)
-        leave(k)
-
-        @pl.when(i == 0)
-        def _():
-            mixer_end()
-            mixes.start()
-
-        @pl.when(i > 0)
-        def _():
-            send_back(i)
-
+    hiddens(nz - 1).relay()
+    mixer_end()
+    mixes.start()
+    leave(nz - 2)
+    leave(nz - 1)
+    send_back(nz - 2)
+    leave(0)
+    send_back(nz - 1)
+    got("sd", "wm")
+
+    shares.finish()
+    routed = 0.0
+    for q in range(tp):
+        routed = routed + dot(r.share[q], r.v_sd[q * sff : (q + 1) * sff, :])
+    r.mixer_sum[...] = dot(r.mix[t], r.v_wm[at(t * width, width), :])
+    mixes.relay()
+    back_pair(0).wait_recv()
+    r.routed_sum[...] = routed + r.ours[0] + r.theirs[0].astype(f32)
+
+    def add_back(k, _):
+        back_in(zsource(k)).wait_recv()
+        r.routed_sum[...] += r.coming[zsource(k)].astype(f32)
         return 0
 
-    lax.fori_loop(0, nz, leaving, 0)
-    mixes.relay()
-    got("sd", "wm")
-
-    back_pair(0).wait_recv()
-    routed = r.ours[0] + r.theirs[0].astype(f32)
-    r.routed_sum[...] = routed + dot(r.mix[t, :, width : width + sff], r.v_sd[at(t * sff, sff), :])
-    r.mixer_sum[...] = dot(r.mix[t, :, 0:width], r.v_wm[at(t * width, width), :])
-    mixes.finish()
-    for q in (tx, ty, td):
-        r.routed_sum[...] += dot(r.mix[q, :, width : width + sff], r.v_sd[at(q * sff, sff), :])
-        r.mixer_sum[...] += dot(r.mix[q, :, 0:width], r.v_wm[at(q * width, width), :])
-    r.mixer_out[...] = r.mixer_sum[...].astype(bf16)
-    total = r.routed_sum[...]
-    for k in range(1, nz):
-        back(k).wait_recv()
-        total = total + r.coming[k].astype(f32)
-    r.routed_out[...] = total.astype(bf16)
+    def add_mix(q):
+        r.mixer_sum[...] += dot(r.mix[q], r.v_wm[at(q * width, width), :])
+
+    def outcopy(i):
+        src, dst = ((r.mixer_bf, r.mixer_out), (r.routed_bf, r.routed_out))[i]
+        return pltpu.make_async_copy(src, dst, r.out_sem.at[i])
+
+    legs = mixes.rest()
+    legs[0].wait_recv()
+    add_mix(tx)
+    legs[1].wait_recv()
+    add_mix(ty)
+    lax.fori_loop(1, nz, add_back, 0)
+    r.routed_bf[...] = r.routed_sum[...].astype(bf16)
+    outcopy(1).start()
+    legs[2].wait_recv()
+    legs[3].wait_recv()
+    add_mix(td)
+    r.mixer_bf[...] = r.mixer_sum[...].astype(bf16)
+    outcopy(0).start()
 
     @pl.when(e + 1 < n_ep)
     def _():
@@ -753,21 +825,39 @@
 
     halves(c).wait_send()
     mixes.drain()
+    shares.drain()
 
     def drain(k, _):
+        source = zsource(k)
+
+        def sent(up):
+            for slot in range(3):
+                along(source, slot, up).wait_send()
+
+        @pl.when(jnp.logical_and(source <= z, onward(1)))
+        def _():
+            sent(1)
+
+        @pl.when(jnp.logical_and(source >= z, onward(0)))
+        def _():
+            sent(0)
+
         @pl.when(k > 0)
         def _():
-            along(k).wait_send()
-            tokens(k).drain()
+            for piece in range(2):
+                for one in token_legs(source, piece):
+                    one.wait_send()
             back(k).wait_send()
 
         for q in range(tp):
-            across(k, q, c).wait_send()
+            across(source, q, c).wait_send()
         hiddens(k).drain()
         back_pair(k).wait_send()
         return 0
 
     lax.fori_loop(0, nz, drain, 0)
+    for i in range(2):
+        outcopy(i).wait()
 
 
 def fused_on_device(*given):
@@ -785,6 +875,8 @@
     cap = max(2, 3 * rows * TOP_K // (2 * local_experts * n_ep))
     for name in ("hld", "skip", "mscale", "scale"):
         argument[name] = argument[name].reshape(1, -1)
+    for name in ("ids", "wts", "step", "extra"):
+        argument[name] = argument[name].T
     dims = types.SimpleNamespace(
         n_ep=n_ep, tp=tp, rows=rows, cap=cap, ratio=heads // groups, quarter=quarter, heads=heads,
         groups=groups, width=width, ff=ff, sff=sff,
@@ -795,7 +887,8 @@
     vmem = dict(
         tok=((n_ep, tp, rows, quarter), bf16),
         hid=((nz, tp, 4 * cap, ff), bf16),
-        mix=((tp, rows, width + sff), bf16),
+        mix=((tp, rows, width), bf16),
+        share=((tp, rows, sff), bf16),
         route=((n_ep, 2 * TOP_K, rows), f32),
         halo_x=((HALO, width), bf16),
         halo_b=((HALO, state_width), bf16),
@@ -832,6 +925,8 @@
         ours=((nz, rows, quarter), f32),
         going=((nz, rows, quarter), bf16),
         coming=((nz, rows, quarter), bf16),
+        routed_bf=((rows, quarter), bf16),
+        mixer_bf=((rows, quarter), bf16),
         routed_sum=((rows, quarter), f32),
         mixer_sum=((rows, quarter), f32),
     )
@@ -839,9 +934,10 @@
         scratch[name] = pltpu.VMEM(shape, dtype)
     sems = dict(
         local_sem=(len(FETCHED),),
-        tok_send=(nz, 6), tok_recv=(nz, 6), hid_send=(nz, 6), hid_recv=(nz, 6),
+        out_sem=(2,),
+        tok_send=(nz, 4), tok_recv=(nz, 4), hid_send=(nz, 6), hid_recv=(nz, 6),
         mix_send=(6,), mix_recv=(6,), pair_send=(nz, tp), pair_recv=(nz, tp),
-        z_send=(nz,), z_recv=(nz,), route_send=(n_ep,), route_recv=(n_ep,),
+        z_send=(nz, 3, 2), z_recv=(nz, 3), share_send=(6,), share_recv=(6,), route_send=(n_ep,), route_recv=(n_ep,),
         halo_send=(3,), halo_recv=(3,), swap_send=(2,), swap_recv=(2,),
         chain_send=(2, nz), chain_recv=(2, nz), half_sem=(2,),
         pair_y_send=(nz,), pair_y_recv=(nz,), y_send=(nz,), y_recv=(nz,),
@@ -856,7 +952,7 @@
             functools.partial(body, dims, names),
             out_shape=(out, out),
             in_specs=[pl.BlockSpec(memory_space=pl.ANY)] * len(order),
-            out_specs=(pl.BlockSpec(memory_space=pltpu.VMEM),) * 2,
+            out_specs=(pl.BlockSpec(memory_space=pl.ANY),) * 2,
             scratch_shapes=list(scratch.values()),
             compiler_params=pltpu.CompilerParams(
                 collective_id=0, has_side_effects=True, vmem_limit_bytes=VMEM_LIMIT
@@ -866,14 +962,14 @@
     )
 
 
-VMEM_LIMIT = 60 * 1024 * 1024
+VMEM_LIMIT = 62 * 1024 * 1024 + 512 * 1024
 ARGUMENTS = (
     "x", "b", "c", "gate", "step", "extra", "hld", "skip", "vk", "bk", "ck", "mscale", "wm",
     "rows", "scale", "ids", "wts", "wg", "wu", "wd", "sg", "su", "sd",
 )
 FETCHED = (
-    "rows", "scale", "ids", "wts", "x", "b", "c", "vk", "bk", "ck", "step", "extra", "hld",
-    "wg", "wu", "sg", "su", "gate", "skip", "mscale", "wd", "sd", "wm",
+    "rows", "scale", "ids", "wts", "x", "b", "c", "sg", "su", "vk", "bk", "ck", "step", "extra", "hld",
+    "wg", "wu", "gate", "skip", "mscale", "wd", "sd", "wm",
 )
 
 

time: 111 us -> 85.2 us (0.77)
  Pallas kernels: 101 us -> 81.1 us
  local copies, waits for them, and re-layouts: 9.24 us -> 3.34 us
    pallas_call x1, Pallas kernels: 101 us -> 81.1 us  [fused_on_device(): pl.pallas_call(functools.partial(body, dims, names), out_shape=(out, out)...]
    unnamed x6 -> x2, local copies, waits for them, and re-layouts: 9.24 us -> 3.34 us
where the time goes in v2:
time: 85.2 us; the launch traced here: 85.1 us
  Pallas kernels  81.1 us (95%)
  local copies, waits for them, and re-layouts  3.34 us (4%)
    pallas_call x1, Pallas kernels, fused_on_device(): pl.pallas_call(functools.partial(body, dims, names), out_shape=(out, out)...  81.1 us
    unnamed x2, local copies, waits for them, and re-layouts  3.34 us

profile of v2, /device:TPU:0, one launch (start us, length us, event | category | flops | bytes accessed | tf_op | source)
XLA Modules:
  0.0 85.1 jit_solution(14012650943074051540)
XLA Ops:
  0.6 81.1 %mixer_and_experts.1 = (bf16[256,512]{1,0:T(8,128)(2,1)}, bf16[256,512]{1,0:T(8,128)(2,1)}) custom-call(bf16[256,2048]{1,0:T(8,128)(2,1)} %refs_0_.1, f32[1,2048]{1,0:T(1,128)} %bitcast.10, s32[4,256]{1,0:T(4,128)} %bitcast.11, f32[4,256]{1,0:T(4,128)} %bitcast.12, bf16[256,1024]{1,0:T(8,128)(2,1)} %refs_4_.1, bf16[256,512]{1,0:T(8,128)(2,1)} %refs_5_.1, ...), custom_call_target="tpu_custom_call" | custom-call | tf_op jit(solution)/shard_map/mixer_and_experts/pallas_call | solution.py:951
  81.7 1.7 %copy.27 = bf16[256,512]{1,0:T(8,128)(2,1)} copy(bf16[256,512]{1,0:T(8,128)(2,1)} %get-tuple-element.4) | data formatting | bytes 524288
  83.4 1.7 %copy.28 = bf16[256,512]{1,0:T(8,128)(2,1)} copy(bf16[256,512]{1,0:T(8,128)(2,1)} %get-tuple-element.5) | data formatting | bytes 524288

commit v3 on v2

--- a/solution.py
+++ b/solution.py
@@ -329,81 +329,70 @@
     for to in (tx, ty):
         pl.semaphore_signal(barrier, inc=1, device_id=(e, to), device_id_type=MESH)
 
-    paired = jnp.minimum(z, nz - 1 - z)
+    longer = jnp.maximum(z, nz - 1 - z)
+    inward = jnp.where(2 * z > nz - 1, -1, 1)
 
     def zsource(k):
-        inward = jnp.where(2 * z > nz - 1, -1, 1)
-        alternate = z + inward * lax.div(k + 1, 2) * (2 * lax.rem(k, 2) - 1)
-        rest = z + inward * (k - paired)
-        return jnp.where(k <= 2 * paired, alternate, rest)
+        return jnp.where(k <= longer, z + inward * k, z - inward * (k - longer))
+
+    def sent(ref, sem):
+        remote(ref, ref, sem, sem, (partner, t)).wait_send()
+
+    def landed(ref, sem):
+        remote(ref, ref, sem, sem, (partner, t)).wait_recv()
 
     def plane(buf, send, recv):
         def leg(q, piece, slot, to):
-            return remote(buf(q, piece), buf(q, piece), send(slot), recv(slot), (e, to))
+            return remote(buf(q, piece), buf(q, piece), send, recv(slot), (e, to))
 
         def start():
             leg(t, 0, 0, tx).start()
-            leg(t, 1, 3, ty).start()
-            leg(t, 1, 1, tx).start()
-            leg(t, 0, 2, ty).start()
+            leg(t, 1, 1, ty).start()
+            leg(t, 1, 2, tx).start()
+            leg(t, 0, 3, ty).start()
 
         def relay():
             leg(tx, 0, 0, tx).wait_recv()
             leg(tx, 0, 4, ty).start()
-            leg(ty, 1, 3, ty).wait_recv()
+            leg(ty, 1, 1, ty).wait_recv()
             leg(ty, 1, 5, tx).start()
 
-        def rest():
-            return leg(tx, 1, 1, tx), leg(ty, 0, 2, ty), leg(td, 0, 4, ty), leg(td, 1, 5, tx)
-
-        def finish():
-            for one in rest():
-                one.wait_recv()
-
-        def drain():
-            leg(t, 0, 0, tx).wait_send()
-            leg(t, 1, 1, tx).wait_send()
-            leg(t, 0, 2, ty).wait_send()
-            leg(t, 1, 3, ty).wait_send()
-            leg(tx, 0, 4, ty).wait_send()
-            leg(ty, 1, 5, tx).wait_send()
-
-        return types.SimpleNamespace(start=start, relay=relay, rest=rest, finish=finish, drain=drain)
+        return types.SimpleNamespace(start=start, relay=relay)
 
     def token_leg(source, q, piece, slot, to):
         ref = r.tok.at[2 * source + c, q, pl.ds(piece * half, half)]
-        return remote(ref, ref, r.tok_send.at[source, slot], r.tok_recv.at[source, slot], (e, to))
+        return remote(ref, ref, r.tok_send, r.tok_recv.at[source, slot], (e, to))
 
     def token_legs(source, piece):
-        return token_leg(source, t, piece, piece, tx), token_leg(source, t, piece, 2 + piece, ty)
+        return token_leg(source, t, piece, 0, tx), token_leg(source, t, piece, 1, ty)
 
     def hiddens(k):
         return plane(
             lambda q, piece: r.hid.at[k, q, pl.ds(piece * 2 * cap, 2 * cap)],
-            lambda slot: r.hid_send.at[k, slot],
-            lambda slot: r.hid_recv.at[k, slot],
+            r.hid_send,
+            lambda slot: r.hid_recv.at[k, min(slot, 2)],
         )
 
     shares = plane(
         lambda q, piece: r.share.at[q, pl.ds(piece * half, half)],
-        lambda slot: r.share_send.at[slot],
-        lambda slot: r.share_recv.at[slot],
+        r.share_send,
+        lambda slot: r.share_recv.at[min(slot, 2)],
     )
     mixes = plane(
         lambda q, piece: r.mix.at[q, pl.ds(piece * half, half)],
-        lambda slot: r.mix_send.at[slot],
-        lambda slot: r.mix_recv.at[slot],
+        r.mix_send,
+        lambda slot: r.mix_recv.at[min(slot, 4)],
     )
 
     def across(source, q, whose):
         ref = r.tok.at[2 * source + whose, q]
-        return remote(ref, ref, r.pair_send.at[source, q], r.pair_recv.at[source, q], (partner, t))
+        return remote(ref, ref, r.pair_send, r.pair_recv.at[source], (partner, t))
 
     def along(source, slot, up):
         block = 2 * source + c
         ref = r.tok.at[block, td] if slot == 2 else r.tok.at[block, t, pl.ds(slot * half, half)]
         to = 2 * (z - 1 + 2 * up) + c
-        return remote(ref, ref, r.z_send.at[source, slot, up], r.z_recv.at[source, slot], (to, t))
+        return remote(ref, ref, r.z_send.at[source, up], r.z_recv.at[source, slot], (to, t))
 
     def onward(up):
         return z + 1 < nz if up else z - 1 >= 0
@@ -444,11 +433,11 @@
 
     def route_to(by):
         ref = r.route.at[e]
-        return remote(ref, ref, r.route_send.at[by], r.route_recv.at[e], (lax.rem(e + by, n_ep), t))
+        return remote(ref, ref, r.route_send, r.route_recv.at[e], (lax.rem(e + by, n_ep), t))
 
     def route_from(source):
         ref = r.route.at[source]
-        return remote(ref, ref, r.route_send.at[0], r.route_recv.at[source], (e, t))
+        return remote(ref, ref, r.route_send, r.route_recv.at[source], (e, t))
 
     edges = ((r.v_x, r.halo_x), (r.v_b, r.halo_b), (r.v_c, r.halo_c))
 
@@ -563,8 +552,7 @@
     conv(r.v_c, r.halo_c, r.v_ck, r.outm)
     route_from(partner).wait_recv()
     got("wg", "wu")
-    for q in range(tp):
-        across(z, q, other).wait_recv()
+    landed(r.tok.at[2 * z + other], r.pair_recv.at[z])
     enter(0)
     hiddens(0).start()
     shares.relay()
@@ -600,16 +588,15 @@
     side = width // 2
     mine_lanes = at(c * side, side)
 
-    def chain(i, by):
-        src, dst = ((r.chip_state, r.chain_state), (r.chip_decay, r.chain_decay))[i]
-        to = 2 * lax.rem(z + by, nz) + c
-        return remote(src, dst.at[z], r.chain_send.at[i, by], r.chain_recv.at[i, z], (to, t))
-
-    def chain_in(i, source):
-        src, dst = ((r.chip_state, r.chain_state), (r.chip_decay, r.chain_decay))[i]
-        return remote(src, dst.at[source], r.chain_send.at[i, 0], r.chain_recv.at[i, source], (e, t))
-
-    def send_chain():
+    def chain(up):
+        to = 2 * (z + up) + c
+        return remote(r.after, r.before, r.chain_sem.at[0], r.chain_sem.at[1], (to, t))
+
+    def halves(whose):
+        ref = r.incoming.at[whose]
+        return remote(ref, ref, r.half_sem.at[0], r.half_sem.at[1], (partner, t))
+
+    def chain_step():
         for i in range(2):
             swap(i).wait_recv()
         ours, theirs = r.state[:, mine_lanes], r.state_in[:, mine_lanes].astype(f32)
@@ -617,14 +604,24 @@
         first = jnp.where(c == 0, ours, theirs)
         second = jnp.where(c == 0, theirs, ours)
         late = jnp.where(c == 0, their_decay, our_decay)
-        r.chip_state[...] = (late[0:1, :] * first + second).astype(bf16)
-        r.chip_decay[...] = our_decay * their_decay
-        for by in range(1, nz):
-
-            @pl.when(z + by < nz)
-            def _():
-                for i in range(2):
-                    chain(i, by).start()
+        chip = late[0:1, :] * first + second
+
+        @pl.when(z == 0)
+        def _():
+            r.before[...] = jnp.zeros_like(r.before)
+
+        @pl.when(z > 0)
+        def _():
+            chain(0).wait_recv()
+
+        r.incoming[c] = r.before[...]
+        halves(c).start()
+
+        @pl.when(onward(1))
+        def _():
+            both = our_decay[0:1, :] * their_decay[0:1, :]
+            r.after[...] = (both * r.before[...].astype(f32) + chip).astype(bf16)
+            chain(1).start()
 
     def inside():
         mid = rows // 2
@@ -647,17 +644,17 @@
                     r.near[span, lanes] = jnp.where(lane, pair[0], pair[1])
 
     def back_pair(k):
-        return remote(r.yours.at[k], r.theirs.at[k], r.pair_y_send.at[k], r.pair_y_recv.at[k], (partner, t))
+        return remote(r.yours.at[k], r.theirs.at[k], r.pair_y_send, r.pair_y_recv.at[k], (partner, t))
 
     def back(k):
         source = zsource(k)
-        return remote(r.going.at[k], r.coming.at[z], r.y_send.at[k], r.y_recv.at[z], (2 * source + c, t))
+        return remote(r.going.at[k], r.coming.at[z], r.y_send, r.y_recv.at[z], (2 * source + c, t))
 
     def back_in(source):
-        return remote(r.going.at[0], r.coming.at[source], r.y_send.at[0], r.y_recv.at[source], (e, t))
+        return remote(r.going.at[0], r.coming.at[source], r.y_send, r.y_recv.at[source], (e, t))
 
     def leave(k, carry=0):
-        hiddens(k).finish()
+        landed(r.hid.at[k, 0:2], r.hid_recv.at[k, 2])
         for j in range(2):
             total = 0.0
             for q in range(tp):
@@ -672,13 +669,46 @@
         r.ours[k] = dot(r.pick[k, c], r.result[c], ((0,), (0,)))
         return carry
 
+    edge = jnp.logical_or(z == 0, z == nz - 1)
+    second = jnp.logical_or(z == 1, z == nz - 2)
+
+    def passing():
+        to = 2 * (z + inward) + c
+        return remote(r.going.at[2], r.passed, r.y_send, r.passed_sem, (to, t))
+
     def send_back(k, carry=0):
-        back_pair(k).wait_recv()
-        r.going[k] = (r.ours[k] + r.theirs[k].astype(f32)).astype(bf16)
-        back(k).start()
+        @pl.when(jnp.logical_not(jnp.logical_and(k == 1, second)))
+        def _():
+            back_pair(k).wait_recv()
+            r.going[k] = (r.ours[k] + r.theirs[k].astype(f32)).astype(bf16)
+            aside = jnp.logical_and(k == 2, edge)
+
+            @pl.when(aside)
+            def _():
+                passing().start()
+
+            @pl.when(jnp.logical_not(aside))
+            def _():
+                back(k).start()
+
         return carry
 
+    def join_back():
+        @pl.when(second)
+        def _():
+            back_pair(1).wait_recv()
+            landed(r.passed, r.passed_sem)
+            total = r.ours[1] + r.theirs[1].astype(f32) + r.passed[...].astype(f32)
+            r.going[1] = total.astype(bf16)
+            back(1).start()
+
+
     sides(1, near_rest)
+
+    @pl.when(z == 0)
+    def _():
+        chain_step()
+
     hiddens(0).relay()
 
     def stage(k, _):
@@ -696,53 +726,38 @@
 
         @pl.when(k == nz - 1)
         def _():
-            send_chain()
-
-        for piece in range(2):
-            token_leg(source, tx, piece, piece, tx).wait_recv()
-        across(source, tx, c).start()
-        for piece in range(2):
-            token_leg(source, ty, piece, 2 + piece, ty).wait_recv()
-        across(source, ty, c).start()
+            hiddens(k - 1).relay()
+
+        for slot, q in ((0, tx), (1, ty)):
+            landed(r.tok.at[2 * source + c, q], r.tok_recv.at[source, slot])
+            across(source, q, c).start()
         for c2 in range(2):
             route_from(2 * source + c2).wait_recv()
 
-        sides(k + 1, near_part)
-        for q in range(tp):
-            across(source, q, other).wait_recv()
+        @pl.when(k != nz - 2)
+        def _():
+            sides(k + 1, near_part)
+
+        @pl.when(k == z)
+        def _():
+            chain_step()
+
+        landed(r.tok.at[2 * source + other], r.pair_recv.at[source])
         enter(k)
+        hiddens(k).start()
+
+        @pl.when(k == nz - 2)
+        def _():
+            sides(k + 1, near_part)
 
         @pl.when(jnp.logical_and(k > 1, k < nz - 1))
         def _():
             hiddens(k - 1).relay()
 
-        hiddens(k).start()
         return 0
 
     lax.fori_loop(1, nz, stage, 0)
-    lax.fori_loop(1, nz - 2, leave, 0)
-    hiddens(nz - 2).relay()
-    lax.fori_loop(1, nz - 2, send_back, 0)
-
-    r.before[...] = jnp.zeros_like(r.before)
-
-    def add_chain(source, _):
-        @pl.when(source < z)
-        def _():
-            for i in range(2):
-                chain_in(i, source).wait_recv()
-            r.before[...] = r.chain_decay[source, 0:1, :] * r.before[...] + r.chain_state[source].astype(f32)
-
-        return 0
-
-    lax.fori_loop(0, nz, add_chain, 0)
-    r.incoming[c] = r.before[...].astype(bf16)
-
-    def halves(whose):
-        ref = r.incoming.at[whose]
-        return remote(ref, ref, r.half_sem.at[0], r.half_sem.at[1], (partner, t))
-
-    halves(c).start()
+
     got("gate", "skip", "mscale")
 
     def mixer_end():
@@ -762,17 +777,19 @@
             by = lax.rsqrt(jnp.mean(gated * gated, axis=-1, keepdims=True) + epsilon)
             r.mix[t, :, lanes] = (gated * by * r.v_mscale[:, lanes]).astype(bf16)
 
+    lax.fori_loop(1, nz - 1, lambda i, carry: leave(nz - 1 - i, carry), 0)
+    send_back(nz - 2)
+    mixer_end()
+    lax.fori_loop(2, nz - 1, lambda i, carry: send_back(nz - 1 - i, carry), 0)
     hiddens(nz - 1).relay()
-    mixer_end()
     mixes.start()
-    leave(nz - 2)
     leave(nz - 1)
-    send_back(nz - 2)
     leave(0)
+    join_back()
     send_back(nz - 1)
     got("sd", "wm")
 
-    shares.finish()
+    landed(r.share.at[0:2], r.share_recv.at[2])
     routed = 0.0
     for q in range(tp):
         routed = routed + dot(r.share[q], r.v_sd[q * sff : (q + 1) * sff, :])
@@ -782,8 +799,15 @@
     r.routed_sum[...] = routed + r.ours[0] + r.theirs[0].astype(f32)
 
     def add_back(k, _):
-        back_in(zsource(k)).wait_recv()
-        r.routed_sum[...] += r.coming[zsource(k)].astype(f32)
+        source = zsource(k)
+        low = jnp.logical_and(source == 0, z == 2)
+        high = jnp.logical_and(source == nz - 1, z == nz - 3)
+
+        @pl.when(jnp.logical_not(jnp.logical_or(low, high)))
+        def _():
+            back_in(source).wait_recv()
+            r.routed_sum[...] += r.coming[source].astype(f32)
+
         return 0
 
     def add_mix(q):
@@ -793,16 +817,14 @@
         src, dst = ((r.mixer_bf, r.mixer_out), (r.routed_bf, r.routed_out))[i]
         return pltpu.make_async_copy(src, dst, r.out_sem.at[i])
 
-    legs = mixes.rest()
-    legs[0].wait_recv()
+    landed(r.mix.at[0, 0:half], r.mix_recv.at[2])
     add_mix(tx)
-    legs[1].wait_recv()
+    landed(r.mix.at[0, 0:half], r.mix_recv.at[3])
     add_mix(ty)
     lax.fori_loop(1, nz, add_back, 0)
     r.routed_bf[...] = r.routed_sum[...].astype(bf16)
     outcopy(1).start()
-    legs[2].wait_recv()
-    legs[3].wait_recv()
+    landed(r.mix.at[0], r.mix_recv.at[4])
     add_mix(td)
     r.mixer_bf[...] = r.mixer_sum[...].astype(bf16)
     outcopy(0).start()
@@ -812,52 +834,68 @@
         for i in range(3):
             halo(i).wait_send()
 
-    for by in range(1, n_ep):
-        route_to(by).wait_send()
+    sent(r.route.at[0 : n_ep - 1], r.route_send)
     for i in range(2):
         swap(i).wait_send()
-    for by in range(1, nz):
-
-        @pl.when(z + by < nz)
-        def _():
-            for i in range(2):
-                chain(i, by).wait_send()
+
+    @pl.when(onward(1))
+    def _():
+        chain(1).wait_send()
 
     halves(c).wait_send()
-    mixes.drain()
-    shares.drain()
-
-    def drain(k, _):
-        source = zsource(k)
-
-        def sent(up):
-            for slot in range(3):
-                along(source, slot, up).wait_send()
-
-        @pl.when(jnp.logical_and(source <= z, onward(1)))
-        def _():
-            sent(1)
-
-        @pl.when(jnp.logical_and(source >= z, onward(0)))
-        def _():
-            sent(0)
-
-        @pl.when(k > 0)
-        def _():
-            for piece in range(2):
-                for one in token_legs(source, piece):
-                    one.wait_send()
-            back(k).wait_send()
-
-        for q in range(tp):
-            across(source, q, c).wait_send()
-        hiddens(k).drain()
-        back_pair(k).wait_send()
+    sent(r.mix.at[0:3], r.mix_send)
+    sent(r.share.at[0:3], r.share_send)
+    sent(r.hid.at[:, 0:3], r.hid_send)
+    sent(r.tok.at[0 : nz - 1, 0:2], r.tok_send)
+    sent(r.tok.at[0:nz], r.pair_send)
+    sent(r.yours, r.pair_y_send)
+    sent(r.going.at[0 : nz - 1], r.y_send)
+
+    def drain(source, _):
+        for up in range(2):
+            passed = source <= z if up else source >= z
+
+            @pl.when(jnp.logical_and(passed, onward(up)))
+            def _():
+                sent(r.tok.at[0, 0:2], r.z_send.at[source, up])
+
         return 0
 
     lax.fori_loop(0, nz, drain, 0)
     for i in range(2):
         outcopy(i).wait()
+
+
+def hand_out_body(first, second, first_out, second_out, held, sems):
+    steps = []
+    for i, (src, dst) in enumerate(((first, first_out), (second, second_out))):
+        steps.append(
+            (
+                pltpu.make_async_copy(src, held.at[i], sems.at[i, 0]),
+                pltpu.make_async_copy(held.at[i], dst, sems.at[i, 1]),
+            )
+        )
+    for arrive, _ in steps:
+        arrive.start()
+    for arrive, depart in steps:
+        arrive.wait()
+        depart.start()
+    for _, depart in steps:
+        depart.wait()
+
+
+def hand_out(first, second):
+    out = jax.ShapeDtypeStruct(first.shape, first.dtype)
+    return tuple(
+        pl.pallas_call(
+            hand_out_body,
+            out_shape=(out, out),
+            in_specs=[pl.BlockSpec(memory_space=pl.ANY)] * 2,
+            out_specs=(pl.BlockSpec(memory_space=pl.ANY),) * 2,
+            scratch_shapes=[pltpu.VMEM((2,) + first.shape, first.dtype), pltpu.SemaphoreType.DMA((2, 2))],
+            name="hand_out",
+        )(first, second)
+    )
 
 
 def fused_on_device(*given):
@@ -907,11 +945,8 @@
         state_in=((STATE, width), bf16),
         decay_out=((8, width), f32),
         decay_in=((8, width), f32),
-        chip_state=((STATE, width // 2), bf16),
-        chip_decay=((8, width // 2), f32),
-        chain_state=((nz, STATE, width // 2), bf16),
-        chain_decay=((nz, 8, width // 2), f32),
-        before=((STATE, width // 2), f32),
+        before=((STATE, width // 2), bf16),
+        after=((STATE, width // 2), bf16),
         incoming=((2, STATE, width // 2), bf16),
         entering=((STATE, width), bf16),
         near=((rows, width), f32),
@@ -925,6 +960,7 @@
         ours=((nz, rows, quarter), f32),
         going=((nz, rows, quarter), bf16),
         coming=((nz, rows, quarter), bf16),
+        passed=((rows, quarter), bf16),
         routed_bf=((rows, quarter), bf16),
         mixer_bf=((rows, quarter), bf16),
         routed_sum=((rows, quarter), f32),
@@ -935,20 +971,20 @@
     sems = dict(
         local_sem=(len(FETCHED),),
         out_sem=(2,),
-        tok_send=(nz, 4), tok_recv=(nz, 4), hid_send=(nz, 6), hid_recv=(nz, 6),
-        mix_send=(6,), mix_recv=(6,), pair_send=(nz, tp), pair_recv=(nz, tp),
-        z_send=(nz, 3, 2), z_recv=(nz, 3), share_send=(6,), share_recv=(6,), route_send=(n_ep,), route_recv=(n_ep,),
+        tok_send=(), tok_recv=(nz, 2), hid_send=(), hid_recv=(nz, 3),
+        mix_send=(), mix_recv=(5,), pair_send=(), pair_recv=(nz,),
+        z_send=(nz, 2), z_recv=(nz, 3), share_send=(), share_recv=(3,), route_send=(), route_recv=(n_ep,),
         halo_send=(3,), halo_recv=(3,), swap_send=(2,), swap_recv=(2,),
-        chain_send=(2, nz), chain_recv=(2, nz), half_sem=(2,),
-        pair_y_send=(nz,), pair_y_recv=(nz,), y_send=(nz,), y_recv=(nz,),
+        chain_sem=(2,), half_sem=(2,), passed_sem=(),
+        pair_y_send=(), pair_y_recv=(nz,), y_send=(), y_recv=(nz,),
     )
     for name, shape in sems.items():
         scratch[name] = pltpu.SemaphoreType.DMA(shape)
     order = tuple(FETCHED)
     names = order + ("mixer_out", "routed_out") + tuple(scratch)
     out = jax.ShapeDtypeStruct((rows, quarter), bf16)
-    return tuple(
-        pl.pallas_call(
+    return hand_out(
+        *pl.pallas_call(
             functools.partial(body, dims, names),
             out_shape=(out, out),
             in_specs=[pl.BlockSpec(memory_space=pl.ANY)] * len(order),
@@ -980,7 +1016,7 @@
     experts = argument["wg"].shape[0]
     cap = max(2, 3 * rows * TOP_K // (2 * experts * n_ep))
     wide = all(argument[n].shape[-1] % LANES == 0 for n in ("x", "b", "wg", "wd", "sg"))
-    fits = tp == 4 and n_ep % 2 == 0 and n_ep >= 6 and experts == 2
+    fits = tp == 4 and n_ep % 2 == 0 and n_ep >= 8 and experts == 2
     fits = fits and wide and cap % 16 == 0 and rows % 32 == 0
     return fused_on_device(*given) if fits else on_device(*given)
 

time: 85.2 us -> 79.8 us (0.937)
  local copies, waits for them, and re-layouts: 3.34 us -> 0 us
  Pallas kernels: 81.1 us -> 79 us
    pallas_call x1, Pallas kernels: 81.1 us -> 77.2 us  [fused_on_device(): pl.pallas_call(functools.partial(body, dims, names), out_shape=(out, out)...]
    unnamed x2 -> x0, local copies, waits for them, and re-layouts: 3.34 us -> none
    pallas_call x0 -> x1, Pallas kernels: none -> 1.77 us  [hand_out(): pl.pallas_call(hand_out_body, out_shape=(out, out), in_specs=[pl.BlockSpe...]
where the time goes in v3:
time: 79.8 us; the launch traced here: 79.7 us
  Pallas kernels  79 us (99%)
    pallas_call x1, Pallas kernels, fused_on_device(): pl.pallas_call(functools.partial(body, dims, names), out_shape=(out, out)...  77.2 us
    pallas_call x1, Pallas kernels, hand_out(): pl.pallas_call(hand_out_body, out_shape=(out, out), in_specs=[pl.BlockSpe...  1.77 us

profile of v3, /device:TPU:0, one launch (start us, length us, event | category | flops | bytes accessed | tf_op | source)
XLA Modules:
  0.0 79.7 jit_solution(14604391274070204684)
XLA Ops:
  0.6 77.2 %mixer_and_experts.1 = (bf16[256,512]{1,0:T(8,128)(2,1)}, bf16[256,512]{1,0:T(8,128)(2,1)}) custom-call(bf16[256,2048]{1,0:T(8,128)(2,1)} %refs_0_.1, f32[1,2048]{1,0:T(1,128)} %bitcast.10, s32[4,256]{1,0:T(4,128)} %bitcast.11, f32[4,256]{1,0:T(4,128)} %bitcast.12, bf16[256,1024]{1,0:T(8,128)(2,1)} %refs_4_.1, bf16[256,512]{1,0:T(8,128)(2,1)} %refs_5_.1, ...), custom_call_target="tpu_custom_call" | custom-call | tf_op jit(solution)/shard_map/mixer_and_experts/pallas_call | solution.py:987
  77.9 1.8 %hand_out.1 = (bf16[256,512]{1,0:T(8,128)(2,1)}, bf16[256,512]{1,0:T(8,128)(2,1)}) custom-call(bf16[256,512]{1,0:T(8,128)(2,1)} %get-tuple-element.4.first, bf16[256,512]{1,0:T(8,128)(2,1)} %get-tuple-element.5.second), custom_call_target="tpu_custom_call" | custom-call | tf_op jit(solution)/shard_map/hand_out/pallas_call | solution.py:890

commit v4 on v3

--- a/solution.py
+++ b/solution.py
@@ -345,11 +345,17 @@
         def leg(q, piece, slot, to):
             return remote(buf(q, piece), buf(q, piece), send, recv(slot), (e, to))
 
-        def start():
+        def lead():
             leg(t, 0, 0, tx).start()
             leg(t, 1, 1, ty).start()
+
+        def follow():
             leg(t, 1, 2, tx).start()
             leg(t, 0, 3, ty).start()
+
+        def start():
+            lead()
+            follow()
 
         def relay():
             leg(tx, 0, 0, tx).wait_recv()
@@ -357,7 +363,7 @@
             leg(ty, 1, 1, ty).wait_recv()
             leg(ty, 1, 5, tx).start()
 
-        return types.SimpleNamespace(start=start, relay=relay)
+        return types.SimpleNamespace(start=start, lead=lead, follow=follow, relay=relay)
 
     def token_leg(source, q, piece, slot, to):
         ref = r.tok.at[2 * source + c, q, pl.ds(piece * half, half)]
@@ -395,16 +401,16 @@
         return remote(ref, ref, r.z_send.at[source, up], r.z_recv.at[source, slot], (to, t))
 
     def onward(up):
-        return z + 1 < nz if up else z - 1 >= 0
+        to = z - 1 + 2 * up
+        return jnp.logical_and(to >= 0, to < nz)
 
     def sides(s, act):
-        @pl.when(z - s >= 0)
-        def _():
-            act(z - s, 1)
-
-        @pl.when(z + s < nz)
-        def _():
-            act(z + s, 0)
+        for way in (1, -1):
+            source = z + way * inward * s
+
+            @pl.when(jnp.logical_and(source >= 0, source < nz))
+            def _(source=source, way=way):
+                act(source, lax.div(1 - way * inward, 2), way)
 
     def pass_on(source, slot, up):
         along(source, slot, 1 - up).wait_recv()
@@ -413,27 +419,38 @@
         def _():
             along(source, slot, up).start()
 
-    def near_piece(piece, source, up):
+    def near_piece(piece, source, up, way):
         pass_on(source, piece, up)
-        for one in token_legs(source, piece):
-            one.start()
-
-    def near_part(source, up):
-        near_piece(0, source, up)
-        near_piece(1, source, up)
-        across(source, t, c).start()
-
-    def near_rest(source, up):
-        near_piece(1, source, up)
-        across(source, t, c).start()
-
-    def far_part(source, up):
+        if way > 0:
+            for one in token_legs(source, piece):
+                one.start()
+
+    def near_rest(source, up, way):
+        near_piece(1, source, up, way)
+        if way > 0:
+            across(source, t, c).start()
+
+    def near_part(source, up, way):
+        near_piece(0, source, up, way)
+        near_rest(source, up, way)
+
+    def late_legs(k):
+        source = zsource(k)
+
+        @pl.when(jnp.logical_and(k > longer, k < nz))
+        def _():
+            for piece in range(2):
+                for one in token_legs(source, piece):
+                    one.start()
+            across(source, t, c).start()
+
+    def far_part(source, up, way):
         pass_on(source, 2, up)
         across(source, td, c).start()
 
-    def route_to(by):
+    def route_to(to):
         ref = r.route.at[e]
-        return remote(ref, ref, r.route_send, r.route_recv.at[e], (lax.rem(e + by, n_ep), t))
+        return remote(ref, ref, r.route_send, r.route_recv.at[e], (to, t))
 
     def route_from(source):
         ref = r.route.at[source]
@@ -473,8 +490,7 @@
         for i in range(3):
             halo(i).start()
 
-    for by in range(1, n_ep):
-        route_to(by).start()
+    route_to(partner).start()
     for slot in range(3):
         for up in (1, 0):
 
@@ -484,6 +500,13 @@
 
     for q in range(tp):
         across(z, q, c).start()
+    for by in range(1, n_ep):
+        to = lax.rem(e + by, n_ep)
+
+        @pl.when(to != partner)
+        def _(to=to):
+            route_to(to).start()
+
     got("sg", "su")
     gate, up = 0.0, 0.0
     for q in range(tp):
@@ -744,11 +767,14 @@
 
         landed(r.tok.at[2 * source + other], r.pair_recv.at[source])
         enter(k)
-        hiddens(k).start()
+        hiddens(k).lead()
 
         @pl.when(k == nz - 2)
         def _():
             sides(k + 1, near_part)
+
+        hiddens(k).follow()
+        late_legs(k + 2)
 
         @pl.when(jnp.logical_and(k > 1, k < nz - 1))
         def _():

time: 79.8 us -> 79.7 us (level)
  no operation moved by 1% of the time
where the time goes in v4:
time: 79.7 us; the launch traced here: 79.6 us
  Pallas kernels  78.9 us (99%)
    pallas_call x1, Pallas kernels, fused_on_device(): pl.pallas_call(functools.partial(body, dims, names), out_shape=(out, out)...  77.1 us
    pallas_call x1, Pallas kernels, hand_out(): pl.pallas_call(hand_out_body, out_shape=(out, out), in_specs=[pl.BlockSpe...  1.77 us

profile of v4, /device:TPU:0, one launch (start us, length us, event | category | flops | bytes accessed | tf_op | source)
XLA Modules:
  0.0 79.6 jit_solution(9486644342128402134)
XLA Ops:
  0.6 77.1 %mixer_and_experts.1 = (bf16[256,512]{1,0:T(8,128)(2,1)}, bf16[256,512]{1,0:T(8,128)(2,1)}) custom-call(bf16[256,2048]{1,0:T(8,128)(2,1)} %refs_0_.1, f32[1,2048]{1,0:T(1,128)} %bitcast.10, s32[4,256]{1,0:T(4,128)} %bitcast.11, f32[4,256]{1,0:T(4,128)} %bitcast.12, bf16[256,1024]{1,0:T(8,128)(2,1)} %refs_4_.1, bf16[256,512]{1,0:T(8,128)(2,1)} %refs_5_.1, ...), custom_call_target="tpu_custom_call" | custom-call | tf_op jit(solution)/shard_map/mixer_and_experts/pallas_call | solution.py:1013
  77.8 1.8 %hand_out.1 = (bf16[256,512]{1,0:T(8,128)(2,1)}, bf16[256,512]{1,0:T(8,128)(2,1)}) custom-call(bf16[256,512]{1,0:T(8,128)(2,1)} %get-tuple-element.4.first, bf16[256,512]{1,0:T(8,128)(2,1)} %get-tuple-element.5.second), custom_call_target="tpu_custom_call" | custom-call | tf_op jit(solution)/shard_map/hand_out/pallas_call | solution.py:916

commit v5 on v4

--- a/solution.py
+++ b/solution.py
@@ -803,12 +803,13 @@
             by = lax.rsqrt(jnp.mean(gated * gated, axis=-1, keepdims=True) + epsilon)
             r.mix[t, :, lanes] = (gated * by * r.v_mscale[:, lanes]).astype(bf16)
 
-    lax.fori_loop(1, nz - 1, lambda i, carry: leave(nz - 1 - i, carry), 0)
-    send_back(nz - 2)
     mixer_end()
-    lax.fori_loop(2, nz - 1, lambda i, carry: send_back(nz - 1 - i, carry), 0)
+    leave(nz - 2)
     hiddens(nz - 1).relay()
     mixes.start()
+    send_back(nz - 2)
+    lax.fori_loop(2, nz - 1, lambda i, carry: leave(nz - 1 - i, carry), 0)
+    lax.fori_loop(2, nz - 1, lambda i, carry: send_back(nz - 1 - i, carry), 0)
     leave(nz - 1)
     leave(0)
     join_back()

time: 79.7 us -> 79 us (level)
  no operation moved by 1% of the time
where the time goes in v5:
time: 79 us; the launch traced here: 78.9 us
  Pallas kernels  78.3 us (99%)
    pallas_call x1, Pallas kernels, fused_on_device(): pl.pallas_call(functools.partial(body, dims, names), out_shape=(out, out)...  76.5 us
    pallas_call x1, Pallas kernels, hand_out(): pl.pallas_call(hand_out_body, out_shape=(out, out), in_specs=[pl.BlockSpe...  1.77 us

profile of v5, /device:TPU:0, one launch (start us, length us, event | category | flops | bytes accessed | tf_op | source)
XLA Modules:
  0.0 78.9 jit_solution(6953187938988718896)
XLA Ops:
  0.6 76.5 %mixer_and_experts.1 = (bf16[256,512]{1,0:T(8,128)(2,1)}, bf16[256,512]{1,0:T(8,128)(2,1)}) custom-call(bf16[256,2048]{1,0:T(8,128)(2,1)} %refs_0_.1, f32[1,2048]{1,0:T(1,128)} %bitcast.10, s32[4,256]{1,0:T(4,128)} %bitcast.11, f32[4,256]{1,0:T(4,128)} %bitcast.12, bf16[256,1024]{1,0:T(8,128)(2,1)} %refs_4_.1, bf16[256,512]{1,0:T(8,128)(2,1)} %refs_5_.1, ...), custom_call_target="tpu_custom_call" | custom-call | tf_op jit(solution)/shard_map/mixer_and_experts/pallas_call | solution.py:1014
  77.1 1.8 %hand_out.1 = (bf16[256,512]{1,0:T(8,128)(2,1)}, bf16[256,512]{1,0:T(8,128)(2,1)}) custom-call(bf16[256,512]{1,0:T(8,128)(2,1)} %get-tuple-element.4.first, bf16[256,512]{1,0:T(8,128)(2,1)} %get-tuple-element.5.second), custom_call_target="tpu_custom_call" | custom-call | tf_op jit(solution)/shard_map/hand_out/pallas_call | solution.py:917
